TPU v7x, 256 devices: a whole 4x4x8 slice. The times are simulated.
256 devices in a mesh: ep: 32 (over z, x), tp: 8 (over y, core).
Axes of the slice: x: 4, y: 4, z: 8, core: 2. Of those that a mesh axis runs over, the one named last changes fastest.
Arguments:
- stream: bfloat16 [512, 4096], P(None, 'ep'), may hold values from -6.5 to 6.5
- norm_gain: float32 [4096], P('ep'), may hold values from 0.1 to 1.9
- w_query: bfloat16 [4096, 2048], P('ep', 'tp'), may hold values from -0.09375 to 0.09375
- w_key: bfloat16 [4096, 1024], P('ep', 'tp'), may hold values from -0.09375 to 0.09375
- w_value: bfloat16 [4096, 1024], P('ep', 'tp'), may hold values from -0.09375 to 0.09375
- break_offset: float32 [16], P('tp'), may hold values from -10 to -2
- cache_keys: bfloat16 [512, 1024, 8, 128], P('ep', None, 'tp'), may hold values from -6 to 6
- cache_values: bfloat16 [512, 1024, 8, 128], P('ep', None, 'tp'), may hold values from -6 to 6
- lengths: int32 [512], P('ep'), may hold values from 128 to 1024
- w_output: bfloat16 [2048, 4096], P('tp', 'ep'), may hold values from -0.125 to 0.125
- head_gain: float32 [2048], P('tp'), may hold values from 0.1 to 1.9
- ffn_gain: float32 [4096], P('ep'), may hold values from 0.1 to 1.9
- route_experts: int32 [512, 2], replicated, may hold values from 0 to 31, all different within a row; in each aligned block of 512 rows (0 to 511, 512 to 1023, ...) at most 64 rows name the same one
- route_weights: float32 [512, 2], replicated, may hold values from 0.1 to 1
- expert_gate: bfloat16 [32, 4096, 1024], P('ep', None, 'tp'), may hold values from -0.09375 to 0.09375
- expert_up: bfloat16 [32, 4096, 1024], P('ep', None, 'tp'), may hold values from -0.09375 to 0.09375
- expert_down: bfloat16 [32, 1024, 4096], P('ep', 'tp'), may hold values from -0.1875 to 0.1875
- dense_gate: bfloat16 [4096, 4096], P('ep', 'tp'), may hold values from -0.09375 to 0.09375
- dense_up: bfloat16 [4096, 4096], P('ep', 'tp'), may hold values from -0.09375 to 0.09375
- dense_down: bfloat16 [4096, 4096], P('tp', 'ep'), may hold values from -0.09375 to 0.09375
- mix_gain: float32 [4096], P('ep'), may hold values from 0.1 to 1.9
Outputs:
- mixed_out: bfloat16 [512, 4096], P(None, 'ep')
- key_rows: bfloat16 [512, 1024], P('ep', 'tp')
- value_rows: bfloat16 [512, 1024], P('ep', 'tp')
Inputs may be any that keep to these rules, and one draw needn't show every extreme that they name: `route_experts`: in the whole batch no expert is named by more than 64 pairs, a bound that some block reaches; the 2 experts of a token differ.
All inputs are finite; a program needn't handle non-finite values.
Results may differ from a plain program's by a relative error of at most 0.025.
Values may be sent and summed in bfloat16 or wider, within the bound.
A program may use at most 64 MiB of HBM per device.

v0:
```python
import jax
import jax.numpy as jnp
from jax import lax
from jax.sharding import PartitionSpec as P

EPSILON = 1e-06


def sent_to_all(x, axis):
    size = lax.axis_size(axis)
    return lax.all_to_all(jnp.broadcast_to(x[None], (size, *x.shape)), axis, 0, 0, tiled=True)


def taken_together(x, axis):
    return sent_to_all(x, axis).sum(axis=0)


def split_up(x, dim, size):
    lengths = x.shape
    blocks = x.reshape(*lengths[:dim], size, lengths[dim] // size, *lengths[dim + 1 :])
    return jnp.moveaxis(blocks, dim, 0)


def sent_and_summed(x, axis, dim):
    blocks = split_up(x, dim, lax.axis_size(axis))
    arrived = lax.all_to_all(blocks, axis, split_axis=0, concat_axis=0, tiled=True)
    return arrived.astype(jnp.float32).sum(axis=0)


def joined_along(blocks, dim):
    blocks = jnp.moveaxis(blocks, 0, dim)
    lengths = blocks.shape
    return blocks.reshape(*lengths[:dim], lengths[dim] * lengths[dim + 1], *lengths[dim + 2 :])


def gather_directly(x, axis, dim):
    return joined_along(sent_to_all(x, axis), dim)


def of_everyone(x, axis):
    return sent_to_all(x, axis).astype(jnp.float32).sum(axis=0)


def rms_scale(values, gain_vec, model_width):
    squares = taken_together(jnp.sum(values * values, axis=1), "ep")
    return values * lax.rsqrt(squares / model_width + EPSILON)[:, None] * gain_vec[None, :]


def to_heads(normed, weights):
    return sent_and_summed(
        jnp.dot(normed, weights, preferred_element_type=jnp.float32).astype(jnp.bfloat16), "ep", 0
    )


def from_heads(values, weights):
    partial_value = jnp.dot(
        gather_directly(values, "ep", 0), weights, preferred_element_type=jnp.float32
    )
    return (
        of_everyone(partial_value.astype(jnp.bfloat16), "tp")
        .astype(jnp.float32)
        .astype(jnp.bfloat16)
    )


def expert_terms(inputs, gate_w, up_w, down_w):
    gate_val = jnp.einsum("ecd,edf->ecf", inputs, gate_w, preferred_element_type=jnp.float32)
    up_val = jnp.einsum("ecd,edf->ecf", inputs, up_w, preferred_element_type=jnp.float32)
    hidden = (jax.nn.silu(gate_val) * up_val).astype(jnp.bfloat16)
    return jnp.einsum("ecf,efd->ecd", hidden, down_w, preferred_element_type=jnp.float32)


def slot_table(route_experts, experts, capacity):
    chosen = route_experts.reshape(-1)
    onehot = (chosen[:, None] == jnp.arange(experts, dtype=jnp.int32)[None, :]).astype(jnp.int32)
    earlier = jnp.cumsum(onehot, axis=0) - onehot
    rank_in = jnp.sum(earlier * onehot, axis=1)
    slot_ids = chosen * capacity + rank_in
    owners = jnp.arange(chosen.shape[0], dtype=jnp.int32) // route_experts.shape[1]
    filled = (
        jnp.full((experts * capacity,), route_experts.shape[0], jnp.int32).at[slot_ids].set(owners)
    )
    return (slot_ids, filled)


def per_device(
    stream,
    norm_gain,
    w_query,
    w_key,
    w_value,
    break_offset,
    cache_keys,
    cache_values,
    lengths,
    w_output,
    head_gain,
    ffn_gain,
    route_experts,
    route_weights,
    expert_gate,
    expert_up,
    expert_down,
    dense_gate,
    dense_up,
    dense_down,
    mix_gain,
):
    model_width = stream.shape[1] * lax.axis_size("ep")
    block_width = stream.shape[1]
    seq_count = lengths.shape[0]
    kv_local = cache_keys.shape[2]
    head_dim = cache_keys.shape[3]
    heads_local = break_offset.shape[0]
    group_size = heads_local // kv_local
    cache_len = cache_keys.shape[1]
    streamf = stream.astype(jnp.float32)
    normed = rms_scale(streamf, norm_gain, model_width).astype(jnp.bfloat16)
    projected = to_heads(normed, jnp.concatenate([w_query, w_key, w_value], axis=1))
    q_width = w_query.shape[1]
    k_width = w_key.shape[1]
    queries = (
        projected[:, :q_width]
        .astype(jnp.bfloat16)
        .reshape(seq_count, kv_local, group_size, head_dim)
    )
    key_rows = projected[:, q_width : q_width + k_width].astype(jnp.bfloat16)
    value_rows = projected[:, q_width + k_width :].astype(jnp.bfloat16)
    scores = jnp.einsum("skgd,slkd->skgl", queries, cache_keys, preferred_element_type=jnp.float32)
    scores = (
        scores * head_dim ** (-0.5) + break_offset.reshape(kv_local, group_size)[None, :, :, None]
    )
    in_cache = (jnp.arange(cache_len, dtype=jnp.int32)[None, :] < lengths[:, None])[
        :, None, None, :
    ]
    failed = jnp.where(in_cache, jax.nn.log_sigmoid(-scores), 0.0)
    later_sum = lax.cumsum(failed, axis=3, reverse=True) - failed
    weights = jnp.where(in_cache, jnp.exp(jax.nn.log_sigmoid(scores) + later_sum), 0.0).astype(
        jnp.bfloat16
    )
    attended = jnp.einsum(
        "skgl,slkd->skgd", weights, cache_values, preferred_element_type=jnp.float32
    )
    gains = head_gain.reshape(kv_local, group_size, head_dim)[None]
    normalized = (
        attended * lax.rsqrt(jnp.mean(attended * attended, axis=3, keepdims=True) + EPSILON) * gains
    )
    head_out = normalized.astype(jnp.bfloat16).reshape(seq_count, heads_local * head_dim)
    attn_out = from_heads(head_out, w_output)
    residual = streamf + attn_out.astype(jnp.float32)
    normed_ffn = rms_scale(residual, ffn_gain, model_width).astype(jnp.bfloat16)
    dense_width = dense_gate.shape[1]
    gate_up = to_heads(normed_ffn, jnp.concatenate([dense_gate, dense_up], axis=1))
    dense_hidden = (jax.nn.silu(gate_up[:, :dense_width]) * gate_up[:, dense_width:]).astype(
        jnp.bfloat16
    )
    dense_out = from_heads(dense_hidden, dense_down)
    experts = expert_gate.shape[0] * lax.axis_size("ep")
    capacity = 2 * seq_count * route_experts.shape[1] // expert_gate.shape[0]
    slot_ids, filled = slot_table(route_experts, experts, capacity)
    padded = jnp.concatenate([normed_ffn, jnp.zeros((1, block_width), jnp.bfloat16)], axis=0)
    outgoing = padded[filled].reshape(experts, capacity, block_width)
    slot_share = capacity // lax.axis_size("tp")
    own_slots = lax.dynamic_slice_in_dim(outgoing, lax.axis_index("tp") * slot_share, slot_share, 1)
    arrived = lax.all_to_all(own_slots, "ep", split_axis=0, concat_axis=2, tiled=True)
    gathered = lax.all_gather(arrived, "tp", axis=1, tiled=True)
    partial_value = expert_terms(gathered, expert_gate, expert_up, expert_down)
    summed = sent_and_summed(partial_value.astype(jnp.bfloat16), "tp", 1).astype(jnp.bfloat16)
    came_back = lax.all_to_all(summed, "ep", split_axis=2, concat_axis=0, tiled=True)
    returned = gather_directly(came_back, "tp", 1)
    picked = returned.reshape(experts * capacity, block_width)[slot_ids]
    picked = picked.reshape(route_experts.shape[0], route_experts.shape[1], block_width).astype(
        jnp.float32
    )
    shares = route_weights / jnp.sum(route_weights, axis=1, keepdims=True)
    moe_out = jnp.sum(picked * shares[:, :, None], axis=1)
    mixed_out = (residual + moe_out + mix_gain[None, :] * dense_out.astype(jnp.float32)).astype(
        jnp.bfloat16
    )
    return (mixed_out, key_rows, value_rows)


def solution(mesh):
    in_specs = (
        P(None, "ep"),
        P("ep"),
        P("ep", "tp"),
        P("ep", "tp"),
        P("ep", "tp"),
        P("tp"),
        P("ep", None, "tp", None),
        P("ep", None, "tp", None),
        P("ep"),
        P("tp", "ep"),
        P("tp"),
        P("ep"),
        P(),
        P(),
        P("ep", None, "tp"),
        P("ep", None, "tp"),
        P("ep", "tp", None),
        P("ep", "tp"),
        P("ep", "tp"),
        P("tp", "ep"),
        P("ep"),
    )
    out_specs = (P(None, "ep"), P("ep", "tp"), P("ep", "tp"))
    return jax.shard_map(
        per_device, mesh=mesh, in_specs=in_specs, out_specs=out_specs, check_vma=False
    )
```

profile of v0, /device:TPU:1, one launch (start us, length us, event | category | flops | bytes accessed | tf_op | source)
XLA Modules:
  0.0 309.1 jit_solution(11907331791318313063)
XLA Ops:
  1.8 20.5 %all_to_all.85 = f32[32,1,512]{2,1,0:T(1,128)S(1)} all-to-all(f32[32,1,512]{2,1,0:T(1,128)S(1)} %broadcast_in_dim.37), channel_id=1, replica_groups=mesh['ep'=32,'tp'=8] {'ep'}, dimensions={0} | all-to-all | bytes 131072 | tf_op jit(solution)/shard_map/all_to_all | solution.py:11
  24.5 3.9 %all-to-all-start.1 = ((bf16[32,16,512]{2,1,0:T(8,128)(2,1)}), bf16[32,16,512]{2,1,0:T(8,128)(2,1)S(1)}, u32[]{:S(2)}, u32[]{:S(2)}) async-start(bf16[32,16,512]{2,1,0:T(8,128)(2,1)} %bitcast), calls=%async_computation.1 | async-start | bytes 1048576 | tf_op jit(solution)/shard_map/all_to_all | solution.py:26
  29.1 14.2 %all-to-all-done.1 = bf16[32,16,512]{2,1,0:T(8,128)(2,1)S(1)} async-done(((bf16[32,16,512]{2,1,0:T(8,128)(2,1)}), bf16[32,16,512]{2,1,0:T(8,128)(2,1)S(1)}, u32[]{:S(2)}, u32[]{:S(2)}) %all-to-all-start.1) | async-done | bytes 524320 | tf_op jit(solution)/shard_map/all_to_all | solution.py:26
  43.4 3.4 %fusion.32 = (f32[16,2,1024]{2,1,0:T(2,128)S(1)}, f32[16,2,1024]{2,1,0:T(2,128)S(1)}) fusion(pred[16,1024]{1,0:T(8,128)(4,1)S(1)} %iota_compare_fusion.2, f32[2]{0:T(128)} %param.26, bf16[16,2,128]{2,1,0:T(2,128)(2,1)S(1)} %reshape.237, bf16[16,1024,1,128]{3,1,2,0:T(8,128)(2,1)} %param.27), kind=kOutput, calls=%fused_computation.44 | convolution fusion | flops 8716288 | bytes 4481032 | tf_op jit(solution)/shard_map/skgd,slkd->skgl/dot_general | solution.py:129
  47.0 39.6 %reduce-window.14 = f32[16,1,2,8,128]{4,3,2,1,0:T(8,128)S(1)} reduce-window(f32[16,1,2,8,128]{4,3,2,1,0:T(8,128)S(1)} %bitcast.111, f32[]{:T(128)} %constant.52.clone.1), window={size=1x1x1x1x128 pad=0_0x0_0x0_0x0_0x0_127}, to_apply=%region_3.4 | reduce-window | flops 4161536 | bytes 262148 | tf_op jit(solution)/shard_map/reduce-window
  87.1 3.3 %multiply_reduce_fusion.1 = (f32[16,2]{1,0:T(8,128)S(1)}, f32[16,2,128]{2,1,0:T(2,128)S(1)}) fusion(bf16[16,1024,1,128]{3,1,2,0:T(8,128)(2,1)} %param.28, pred[16,1024]{1,0:T(8,128)(4,1)S(1)} %iota_compare_fusion.2, f32[16,2,1024]{2,1,0:T(2,128)S(1)} %reshape.240, f32[16,2,1024]{2,1,0:T(2,128)S(1)} %reshape.243, f32[16,2,1024]{2,1,0:T(2,128)S(1)} %get-tuple-element.6), kind=kOutput, calls=%fused_computation.75 | convolution fusion | flops 9084896 | bytes 4620416 | tf_op jit(solution)/shard_map/skgl,slkd->skgd/dot_general | solution.py:141
  91.3 6.3 %all-to-all-start.2 = ((bf16[32,16,256]{2,1,0:T(8,128)(2,1)}), bf16[32,16,256]{2,1,0:T(8,128)(2,1)S(1)}, u32[]{:S(2)}, u32[]{:S(2)}) async-start(bf16[32,16,256]{2,1,0:T(8,128)(2,1)} %broadcast_in_dim.39), calls=%async_computation.2 | async-start | bytes 524288 | tf_op jit(solution)/shard_map/all_to_all | solution.py:11
  98.0 10.1 %all-to-all-done.2 = bf16[32,16,256]{2,1,0:T(8,128)(2,1)S(1)} async-done(((bf16[32,16,256]{2,1,0:T(8,128)(2,1)}), bf16[32,16,256]{2,1,0:T(8,128)(2,1)S(1)}, u32[]{:S(2)}, u32[]{:S(2)}) %all-to-all-start.2) | async-done | bytes 262176 | tf_op jit(solution)/shard_map/all_to_all | solution.py:11
  109.4 8.2 %all-to-all-start.3 = ((bf16[8,512,128]{2,1,0:T(8,128)(2,1)}), bf16[8,512,128]{2,1,0:T(8,128)(2,1)S(1)}, u32[]{:S(2)}, u32[]{:S(2)}) async-start(bf16[8,512,128]{2,1,0:T(8,128)(2,1)} %broadcast_in_dim.40), calls=%async_computation.3 | async-start | bytes 2097152 | tf_op jit(solution)/shard_map/all_to_all | solution.py:11
  117.8 9.0 %reduce-window.16 = s32[32,8,128]{2,1,0:T(8,128)S(1)} reduce-window(s32[32,8,128]{2,1,0:T(8,128)S(1)} %fusion.43, s32[]{:T(128)} %constant.60.clone.1), window={size=1x1x128 pad=0_0x0_0x127_0}, to_apply=%region_9.10 | reduce-window | flops 4161536 | bytes 262148 | tf_op jit(solution)/shard_map/reduce-window.2
  127.7 4.3 %scatter_custom_fusion = s32[2048]{0:T(1024)S(1)} fusion(s32[1024]{0:T(1024)S(1)} %bitcast.121, s32[1024]{0:T(1024)S(1)} %add_select_fusion, s32[]{:T(128)} %constant.58.clone.1), kind=kCustom, calls=%fused_computation.86 | custom fusion | bytes 8196 | tf_op jit(solution)/shard_map/scatter | solution.py:81
  133.6 3.9 %all-to-all-start.4 = ((f32[32,1,512]{2,1,0:T(1,128)}), f32[32,1,512]{2,1,0:T(1,128)S(1)}, u32[]{:S(2)}, u32[]{:S(2)}) async-start(f32[32,1,512]{2,1,0:T(1,128)} %broadcast_in_dim.41), calls=%async_computation.4 | async-start | bytes 131072 | tf_op jit(solution)/shard_map/all_to_all | solution.py:11
  137.4 8.9 %all-to-all-done.4 = f32[32,1,512]{2,1,0:T(1,128)S(1)} async-done(((f32[32,1,512]{2,1,0:T(1,128)}), f32[32,1,512]{2,1,0:T(1,128)S(1)}, u32[]{:S(2)}, u32[]{:S(2)}) %all-to-all-start.4) | async-done | bytes 65568 | tf_op jit(solution)/shard_map/all_to_all | solution.py:11
  146.5 6.2 %gather_fusion = bf16[2048,128]{1,0:T(8,128)(2,1)S(1)} fusion(bf16[513,128]{1,0:T(8,128)(2,1)S(1)} %concatenate.10, s32[2048]{0:T(1024)S(1)} %fusion.52), kind=kCustom, calls=%fused_computation | custom fusion | bytes 1056768 | tf_op jit(solution)/shard_map/gather | solution.py:162
  152.8 12.0 %all_to_all.86 = bf16[32,8,128]{2,1,0:T(8,128)(2,1)S(1)} all-to-all(bf16[32,8,128]{2,1,0:T(8,128)(2,1)S(1)} %constant_dynamic-slice_fusion), channel_id=1, replica_groups=mesh['ep'=32,'tp'=8] {'ep'}, dimensions={0} | all-to-all | bytes 131072 | tf_op jit(solution)/shard_map/all_to_all | solution.py:165
  164.8 16.2 %all_gather.3 = bf16[1,64,4096]{2,1,0:T(8,128)(2,1)S(1)} all-gather(bf16[1,8,4096]{2,1,0:T(8,128)(2,1)S(1)} %bitcast.112), channel_id=1, replica_groups=mesh['ep'=32,'tp'=8] {'tp'}, dimensions={1}, use_global_device_ids=true | all-gather | bytes 589824 | tf_op jit(solution)/shard_map/all_gather | solution.py:166
  183.9 3.6 %all-to-all-start.6 = ((bf16[8,1,8,4096]{3,2,1,0:T(8,128)(2,1)}), bf16[8,1,8,4096]{3,2,1,0:T(8,128)(2,1)S(1)}, u32[]{:S(2)}, u32[]{:S(2)}) async-start(bf16[8,1,8,4096]{3,2,1,0:T(8,128)(2,1)} %fusion), calls=%async_computation.6 | async-start | bytes 1048576 | tf_op jit(solution)/shard_map/all_to_all | solution.py:26
  188.9 8.0 %all-to-all-done.6 = bf16[8,1,8,4096]{3,2,1,0:T(8,128)(2,1)S(1)} async-done(((bf16[8,1,8,4096]{3,2,1,0:T(8,128)(2,1)}), bf16[8,1,8,4096]{3,2,1,0:T(8,128)(2,1)S(1)}, u32[]{:S(2)}, u32[]{:S(2)}) %all-to-all-start.6) | async-done | bytes 524320 | tf_op jit(solution)/shard_map/all_to_all | solution.py:26
  196.9 4.8 %all-to-all-start.9 = ((bf16[32,16,1024]{2,1,0:T(8,128)(2,1)}), bf16[32,16,1024]{2,1,0:T(8,128)(2,1)}, u32[]{:S(2)}, u32[]{:S(2)}) async-start(bf16[32,16,1024]{2,1,0:T(8,128)(2,1)} %bitcast.28), calls=%async_computation.9 | async-start | bytes 2097152 | tf_op jit(solution)/shard_map/all_to_all | solution.py:26
  205.1 23.4 %reduce.9 = bf16[4096,8]{1,0:T(8,128)(2,1)} reduce(bf16[4096,1,8]{2,1,0:T(2,128)(2,1)S(1)} %bitcast.103, bf16[]{:T(256)} %broadcast.165), dimensions={1}, to_apply=%bitcast.86.reduce_sub_computation | reduce | bytes 131074
  228.5 3.1 reshape.282
  231.6 9.1 %all-to-all-start.7 = ((bf16[32,2,512]{2,1,0:T(2,128)(2,1)}), bf16[32,2,512]{2,1,0:T(2,128)(2,1)S(1)}, u32[]{:S(2)}, u32[]{:S(2)}) async-start(bf16[32,2,512]{2,1,0:T(2,128)(2,1)} %reshape.282), calls=%async_computation.7 | async-start | bytes 131072 | tf_op jit(solution)/shard_map/all_to_all | solution.py:169
  242.2 7.4 %all-to-all-done.7 = bf16[32,2,512]{2,1,0:T(2,128)(2,1)S(1)} async-done(((bf16[32,2,512]{2,1,0:T(2,128)(2,1)}), bf16[32,2,512]{2,1,0:T(2,128)(2,1)S(1)}, u32[]{:S(2)}, u32[]{:S(2)}) %all-to-all-start.7) | async-done | bytes 65568 | tf_op jit(solution)/shard_map/all_to_all | solution.py:169
  250.4 4.6 %all-to-all-start.10 = ((bf16[32,16,512]{2,1,0:T(8,128)(2,1)}), bf16[32,16,512]{2,1,0:T(8,128)(2,1)}, u32[]{:S(2)}, u32[]{:S(2)}) async-start(bf16[32,16,512]{2,1,0:T(8,128)(2,1)} %broadcast_in_dim.46), calls=%async_computation.10 | async-start | bytes 1048576 | tf_op jit(solution)/shard_map/all_to_all | solution.py:11
  255.1 2.8 reshape.283
  259.8 9.4 %all-to-all-done.10 = bf16[32,16,512]{2,1,0:T(8,128)(2,1)} async-done(((bf16[32,16,512]{2,1,0:T(8,128)(2,1)}), bf16[32,16,512]{2,1,0:T(8,128)(2,1)}, u32[]{:S(2)}, u32[]{:S(2)}) %all-to-all-start.10) | async-done | bytes 524320 | tf_op jit(solution)/shard_map/all_to_all | solution.py:11
  270.1 8.2 %all-to-all-start.8 = ((bf16[8,32,8,128]{3,2,1,0:T(8,128)(2,1)}), bf16[8,32,8,128]{3,2,1,0:T(8,128)(2,1)S(1)}, u32[]{:S(2)}, u32[]{:S(2)}) async-start(bf16[8,32,8,128]{3,2,1,0:T(8,128)(2,1)} %broadcast_in_dim.45), calls=%async_computation.8 | async-start | bytes 1048576 | tf_op jit(solution)/shard_map/all_to_all | solution.py:11
  279.6 8.0 %all-to-all-done.8 = bf16[8,32,8,128]{3,2,1,0:T(8,128)(2,1)S(1)} async-done(((bf16[8,32,8,128]{3,2,1,0:T(8,128)(2,1)}), bf16[8,32,8,128]{3,2,1,0:T(8,128)(2,1)S(1)}, u32[]{:S(2)}, u32[]{:S(2)}) %all-to-all-start.8) | async-done | bytes 524320 | tf_op jit(solution)/shard_map/all_to_all | solution.py:11
  288.8 4.4 %all-to-all-start.11 = ((bf16[8,512,128]{2,1,0:T(8,128)(2,1)}), bf16[8,512,128]{2,1,0:T(8,128)(2,1)S(1)}, u32[]{:S(2)}, u32[]{:S(2)}) async-start(bf16[8,512,128]{2,1,0:T(8,128)(2,1)} %broadcast_in_dim.47), calls=%async_computation.11 | async-start | bytes 2097152 | tf_op jit(solution)/shard_map/all_to_all | solution.py:11
  294.9 3.2 %gather_fusion.1 = bf16[1024,128]{1,0:T(8,128)(2,1)S(1)} fusion(bf16[2048,128]{1,0:T(8,128)(2,1)S(1)} %bitcast.102, s32[1024]{0:T(1024)S(1)} %broadcast_clamp_fusion), kind=kCustom, calls=%fused_computation.1 | custom fusion | bytes 528384 | tf_op jit(solution)/shard_map/gather | solution.py:171
  298.1 3.7 %fusion.17 = f32[512,128]{1,0:T(8,128)S(1)} fusion(bf16[512,2,128]{2,1,0:T(2,128)(2,1)S(1)} %bitcast.107, f32[512,2]{1,0:T(8,128)} %copy.90), kind=kLoop, calls=%fused_computation.23 | loop fusion | flops 327680 | bytes 528384 | tf_op jit(solution)/shard_map/reduce_sum | solution.py:176
  301.8 6.4 %all-to-all-done.11 = bf16[8,512,128]{2,1,0:T(8,128)(2,1)S(1)} async-done(((bf16[8,512,128]{2,1,0:T(8,128)(2,1)}), bf16[8,512,128]{2,1,0:T(8,128)(2,1)S(1)}, u32[]{:S(2)}, u32[]{:S(2)}) %all-to-all-start.11) | async-done | bytes 1048608 | tf_op jit(solution)/shard_map/all_to_all | solution.py:11
  (95 shorter events, 27.9 us)
Async XLA Ops:
  0.6 181.9 %copy-start = (bf16[1,128,4096]{2,1,0:T(8,128)(2,1)S(1)}, bf16[1,128,4096]{2,1,0:T(8,128)(2,1)}, u32[]{:S(2)}) copy-start(bf16[1,128,4096]{2,1,0:T(8,128)(2,1)} %param.37) | copy-start | bytes 3145732
  24.5 18.8 %all-to-all-start.1 = ((bf16[32,16,512]{2,1,0:T(8,128)(2,1)}), bf16[32,16,512]{2,1,0:T(8,128)(2,1)S(1)}, u32[]{:S(2)}, u32[]{:S(2)}) async-start(bf16[32,16,512]{2,1,0:T(8,128)(2,1)} %bitcast), calls=%async_computation.1 | async-start | bytes 1048576 | tf_op jit(solution)/shard_map/all_to_all | solution.py:26
  46.8 43.6 %copy-start.8 = (f32[256]{0:T(256)S(1)}, f32[256]{0:T(256)}, u32[]{:S(2)}) copy-start(f32[256]{0:T(256)} %param.31) | copy-start | bytes 3076
  46.8 50.8 %copy-start.6 = (s32[512,2]{0,1:T(2,128)S(1)}, s32[512,2]{0,1:T(2,128)}, u32[]{:S(2)}) copy-start(s32[512,2]{0,1:T(2,128)} %param.33) | copy-start | bytes 12292
  46.9 61.1 %copy-start.5 = (bf16[256,128]{1,0:T(8,128)(2,1)S(1)}, bf16[256,128]{1,0:T(8,128)(2,1)}, u32[]{:S(2)}) copy-start(bf16[256,128]{1,0:T(8,128)(2,1)} %param.30) | copy-start | bytes 196612
  90.5 42.2 %copy-start.1 = (bf16[512,128]{1,0:T(8,128)(2,1)S(1)}, bf16[512,128]{1,0:T(8,128)(2,1)}, u32[]{:S(2)}) copy-start(bf16[512,128]{1,0:T(8,128)(2,1)} %param.21) | copy-start | bytes 393220
  91.3 55.1 %copy-start.9 = (f32[128]{0:T(128)S(1)}, f32[128]{0:T(128)}, u32[]{:S(2)}) copy-start(f32[128]{0:T(128)} %param.32) | copy-start | bytes 1540
  91.3 16.7 %all-to-all-start.2 = ((bf16[32,16,256]{2,1,0:T(8,128)(2,1)}), bf16[32,16,256]{2,1,0:T(8,128)(2,1)S(1)}, u32[]{:S(2)}, u32[]{:S(2)}) async-start(bf16[32,16,256]{2,1,0:T(8,128)(2,1)} %broadcast_in_dim.39), calls=%async_computation.2 | async-start | bytes 524288 | tf_op jit(solution)/shard_map/all_to_all | solution.py:11
  109.4 23.2 %all-to-all-start.3 = ((bf16[8,512,128]{2,1,0:T(8,128)(2,1)}), bf16[8,512,128]{2,1,0:T(8,128)(2,1)S(1)}, u32[]{:S(2)}, u32[]{:S(2)}) async-start(bf16[8,512,128]{2,1,0:T(8,128)(2,1)} %broadcast_in_dim.40), calls=%async_computation.3 | async-start | bytes 2097152 | tf_op jit(solution)/shard_map/all_to_all | solution.py:11
  132.7 49.8 %copy-start.2 = (bf16[1,4096,128]{2,1,0:T(8,128)(2,1)S(1)}, bf16[1,4096,128]{2,1,0:T(8,128)(2,1)}, u32[]{:S(2)}) copy-start(bf16[1,4096,128]{2,1,0:T(8,128)(2,1)} %param.36) | copy-start | bytes 3145732
  133.6 12.7 %all-to-all-start.4 = ((f32[32,1,512]{2,1,0:T(1,128)}), f32[32,1,512]{2,1,0:T(1,128)S(1)}, u32[]{:S(2)}, u32[]{:S(2)}) async-start(f32[32,1,512]{2,1,0:T(1,128)} %broadcast_in_dim.41), calls=%async_computation.4 | async-start | bytes 131072 | tf_op jit(solution)/shard_map/all_to_all | solution.py:11
  152.7 34.8 %copy-start.3 = (bf16[128,512]{1,0:T(8,128)(2,1)S(1)}, bf16[128,512]{1,0:T(8,128)(2,1)}, u32[]{:S(2)}) copy-start(bf16[128,512]{1,0:T(8,128)(2,1)} %param.39) | copy-start | bytes 393220
  152.7 34.8 %copy-start.4 = (bf16[128,512]{1,0:T(8,128)(2,1)S(1)}, bf16[128,512]{1,0:T(8,128)(2,1)}, u32[]{:S(2)}) copy-start(bf16[128,512]{1,0:T(8,128)(2,1)} %param.38) | copy-start | bytes 393220
  183.9 12.9 %all-to-all-start.6 = ((bf16[8,1,8,4096]{3,2,1,0:T(8,128)(2,1)}), bf16[8,1,8,4096]{3,2,1,0:T(8,128)(2,1)S(1)}, u32[]{:S(2)}, u32[]{:S(2)}) async-start(bf16[8,1,8,4096]{3,2,1,0:T(8,128)(2,1)} %fusion), calls=%async_computation.6 | async-start | bytes 1048576 | tf_op jit(solution)/shard_map/all_to_all | solution.py:26
  196.9 34.7 %all-to-all-start.9 = ((bf16[32,16,1024]{2,1,0:T(8,128)(2,1)}), bf16[32,16,1024]{2,1,0:T(8,128)(2,1)}, u32[]{:S(2)}, u32[]{:S(2)}) async-start(bf16[32,16,1024]{2,1,0:T(8,128)(2,1)} %bitcast.28), calls=%async_computation.9 | async-start | bytes 2097152 | tf_op jit(solution)/shard_map/all_to_all | solution.py:26
  231.6 18.0 %all-to-all-start.7 = ((bf16[32,2,512]{2,1,0:T(2,128)(2,1)}), bf16[32,2,512]{2,1,0:T(2,128)(2,1)S(1)}, u32[]{:S(2)}, u32[]{:S(2)}) async-start(bf16[32,2,512]{2,1,0:T(2,128)(2,1)} %reshape.282), calls=%async_computation.7 | async-start | bytes 131072 | tf_op jit(solution)/shard_map/all_to_all | solution.py:169
  250.4 18.8 %all-to-all-start.10 = ((bf16[32,16,512]{2,1,0:T(8,128)(2,1)}), bf16[32,16,512]{2,1,0:T(8,128)(2,1)}, u32[]{:S(2)}, u32[]{:S(2)}) async-start(bf16[32,16,512]{2,1,0:T(8,128)(2,1)} %broadcast_in_dim.46), calls=%async_computation.10 | async-start | bytes 1048576 | tf_op jit(solution)/shard_map/all_to_all | solution.py:11
  257.9 35.4 %copy-start.7 = (f32[512,2]{0,1:T(2,128)S(1)}, f32[512,2]{0,1:T(2,128)}, u32[]{:S(2)}) copy-start(f32[512,2]{0,1:T(2,128)} %param.34) | copy-start | bytes 12292
  270.1 17.6 %all-to-all-start.8 = ((bf16[8,32,8,128]{3,2,1,0:T(8,128)(2,1)}), bf16[8,32,8,128]{3,2,1,0:T(8,128)(2,1)S(1)}, u32[]{:S(2)}, u32[]{:S(2)}) async-start(bf16[8,32,8,128]{3,2,1,0:T(8,128)(2,1)} %broadcast_in_dim.45), calls=%async_computation.8 | async-start | bytes 1048576 | tf_op jit(solution)/shard_map/all_to_all | solution.py:11
  279.6 28.7 %copy-start.10 = (f32[128]{0:T(128)S(1)}, f32[128]{0:T(128)}, u32[]{:S(2)}) copy-start(f32[128]{0:T(128)} %param.41) | copy-start | bytes 1540
  288.8 19.4 %all-to-all-start.11 = ((bf16[8,512,128]{2,1,0:T(8,128)(2,1)}), bf16[8,512,128]{2,1,0:T(8,128)(2,1)S(1)}, u32[]{:S(2)}, u32[]{:S(2)}) async-start(bf16[8,512,128]{2,1,0:T(8,128)(2,1)} %broadcast_in_dim.47), calls=%async_computation.11 | async-start | bytes 2097152 | tf_op jit(solution)/shard_map/all_to_all | solution.py:11
where the time goes:
time: 310 us; the launch traced here: 309 us
  other arithmetic  81 us (26%)
  waiting for transfers between devices  72.8 us (23%)
  starting transfers between devices  57.1 us (18%)
  blocking collectives  48.7 us (16%)
  local copies, waits for them, and re-layouts  33.7 us (11%)
  matrix products  14.7 us (5%)
    another operation x5, other arithmetic  48.8 us
    all_to_all x6, waiting for transfers between devices, sent_to_all(): lax.all_to_all(jnp.broadcast_to(x[None], (size, *x.shape)), axis, 0, 0, t...  43.3 us
    all_to_all x6, starting transfers between devices, sent_to_all(): lax.all_to_all(jnp.broadcast_to(x[None], (size, *x.shape)), axis, 0, 0, t...  35.6 us
    unnamed x1, other arithmetic  23.4 us
    all_to_all x3, waiting for transfers between devices, sent_and_summed(): lax.all_to_all(blocks, axis, split_axis=0, concat_axis=0, tiled=True)  22.1 us
    all_to_all x1, blocking collectives, sent_to_all(): lax.all_to_all(jnp.broadcast_to(x[None], (size, *x.shape)), axis, 0, 0, t...  20.5 us
    all_gather x1, blocking collectives, per_device(): gathered = lax.all_gather(arrived, 'tp', axis=1, tiled=True)  16.2 us
    all_to_all x3, starting transfers between devices, sent_and_summed(): lax.all_to_all(blocks, axis, split_axis=0, concat_axis=0, tiled=True)  12.3 us
  transfers between devices with their start and end apart: 10, of which 9 were waited for; matrix products, arithmetic and copies ran while one was open for 20% of the time, Pallas kernels for 0%

commit v1 on v0

--- a/solution.py
+++ b/solution.py
@@ -1,9 +1,246 @@
+import functools
+
 import jax
 import jax.numpy as jnp
 from jax import lax
+from jax.experimental import pallas as pl
+from jax.experimental.pallas import tpu as pltpu
 from jax.sharding import PartitionSpec as P
 
 EPSILON = 1e-06
+NX, NZ, NT = 4, 8, 8
+MODEL, HD, LEN, ROWS = 4096, 128, 1024, 16
+F32, BF16 = jnp.float32, jnp.bfloat16
+HIGH = lax.Precision.HIGHEST
+
+
+def iota(shape, dim):
+    return lax.broadcasted_iota(jnp.int32, shape, dim)
+
+
+def front_kernel(
+    stream, wq, wk, wv, ck, cv, wo, ngain, hgain, boff, lens,
+    attn_out, key_rows, value_rows,
+    strm, wqkv, kbuf, vbuf, ybuf, yrecv, ssq, ssqr, zbuf, zrecv, zsq, zsqr,
+    wog, hall, obuf, orecv, abuf, agath,
+    lsem, ssem,
+    yx_sem, sx_sem, wo_sem, yz_sem, sz_sem, h_sem, o_sem, a_sem,
+):
+    e = lax.axis_index("ep")
+    t = lax.axis_index("tp")
+    z = lax.div(e, NX)
+    x = lax.rem(e, NX)
+
+    def at_x(d):
+        return lax.rem(x + d, NX)
+
+    def at_z(d):
+        return lax.rem(z + d, NZ)
+
+    def at_t(d):
+        return lax.rem(t + d, NT)
+
+    started = []
+
+    def send(src, dst, rsem, dev_e, dev_t):
+        copy = pltpu.make_async_remote_copy(
+            src_ref=src, dst_ref=dst, send_sem=ssem.at[len(started)], recv_sem=rsem,
+            device_id=(dev_e, dev_t), device_id_type=pl.DeviceIdType.MESH,
+        )
+        copy.start()
+        started.append(copy)
+
+    def arrived(dst, rsem):
+        pltpu.make_async_copy(dst, dst, rsem).wait()
+
+    local = []
+
+    def load(src, dst):
+        copy = pltpu.make_async_copy(src, dst, lsem.at[len(local)])
+        copy.start()
+        local.append(copy)
+        return copy
+
+    c_w = [load(wq, wqkv.at[:, 0:256]), load(wk, wqkv.at[:, 256:384]), load(wv, wqkv.at[:, 384:512])]
+    c_s = [load(stream.at[:, xi], strm.at[xi]) for xi in range(NX)]
+
+    barrier = pltpu.get_barrier_semaphore()
+    peers = 0
+    for dz in range(NZ):
+        for dx in range(NX):
+            if dz == 0 or dx == 0:
+                if dz or dx:
+                    pl.semaphore_signal(barrier, inc=1, device_id=(at_z(dz) * NX + at_x(dx), t), device_id_type=pl.DeviceIdType.MESH)
+                    peers += 1
+    for dt in range(1, NT):
+        for dx in range(NX):
+            pl.semaphore_signal(barrier, inc=1, device_id=(z * NX + at_x(dx), at_t(dt)), device_id_type=pl.DeviceIdType.MESH)
+            peers += 1
+
+    c_k = load(ck, kbuf)
+    c_v = load(cv, vbuf)
+    c_wo = load(wo, wog.at[x])
+
+    for c in c_w + c_s:
+        c.wait()
+    gain = ngain[...]
+    w = wqkv[...]
+    for xi in range(NX):
+        rows = strm[xi].reshape(NZ * ROWS, HD).astype(F32)
+        ybuf[xi] = jnp.dot((rows * gain).astype(BF16), w, preferred_element_type=F32).astype(BF16)
+        sums = jnp.sum((rows * rows).T, axis=0, keepdims=True)
+        ssq[xi] = jnp.broadcast_to(sums, (8, HD))
+
+    pl.semaphore_wait(barrier, peers)
+
+    for d in (2, 1, 3):
+        to = z * NX + at_x(d)
+        send(ybuf.at[at_x(d)], yrecv.at[d - 1], yx_sem.at[d - 1], to, t)
+        send(ssq.at[at_x(d)], ssqr.at[d - 1], sx_sem.at[d - 1], to, t)
+    c_wo.wait()
+    for d in (2, 1, 3):
+        send(wog.at[x], wog.at[x], wo_sem.at[d - 1], z * NX + at_x(d), t)
+    total = ybuf[x].astype(F32)
+    sq = ssq[x]
+    for d in (1, 3, 2):
+        arrived(yrecv.at[d - 1], yx_sem.at[d - 1])
+        arrived(ssqr.at[d - 1], sx_sem.at[d - 1])
+        total = total + yrecv[d - 1].astype(F32)
+        sq = sq + ssqr[d - 1]
+    zbuf[...] = total.astype(BF16).reshape(NZ, ROWS, 512)
+    zsq[...] = sq
+
+    for d in (4, 3, 5, 2, 6, 1, 7):
+        to = at_z(d) * NX + x
+        send(zbuf.at[at_z(d)], zrecv.at[d - 1], yz_sem.at[d - 1], to, t)
+        send(zsq, zsqr.at[d - 1], sz_sem.at[d - 1], to, t)
+    qkv = zbuf[z].astype(F32)
+    sq = zsq[...]
+    for d in (1, 7, 2, 6, 3, 5, 4):
+        arrived(zrecv.at[d - 1], yz_sem.at[d - 1])
+        arrived(zsqr.at[d - 1], sz_sem.at[d - 1])
+        qkv = qkv + zrecv[d - 1].astype(F32)
+        sq = sq + zsqr[d - 1]
+    lane = iota((ROWS, HD), 1)
+    pick = lane == z * ROWS + iota((ROWS, HD), 0)
+    mean = jnp.sum(jnp.where(pick, jnp.broadcast_to(sq[0:1], (ROWS, HD)), 0.0), axis=1, keepdims=True) / MODEL
+    qkv = qkv * lax.rsqrt(mean + EPSILON)
+    key_rows[...] = qkv[:, 256:384].astype(BF16)
+    value_rows[...] = qkv[:, 384:512].astype(BF16)
+
+    q = jnp.concatenate([qkv[:, 0:128], qkv[:, 128:256]], axis=0).astype(BF16).astype(F32)
+    seq = lax.rem(iota((2 * ROWS, 1), 0), ROWS)
+    c_k.wait()
+    scores = jnp.zeros((2 * ROWS, LEN), F32)
+    for p in range(ROWS // 2):
+        keys = jnp.concatenate([kbuf[2 * p], kbuf[2 * p + 1]], axis=1)
+        own = jnp.concatenate([jnp.where(seq == 2 * p, q, 0.0), jnp.where(seq == 2 * p + 1, q, 0.0)], axis=1)
+        scores = scores + lax.dot_general(own.astype(BF16), keys, (((1,), (1,)), ((), ())), preferred_element_type=F32)
+    first = iota((2 * ROWS, 1), 0) < ROWS
+    length = jnp.zeros((2 * ROWS, 1), jnp.int32)
+    for s in range(ROWS):
+        length = jnp.where(seq == s, lens[s], length)
+    scores = scores * HD ** (-0.5) + jnp.where(first, boff[0], boff[1])
+    inside = iota((2 * ROWS, LEN), 1) < length
+    tail = jnp.log1p(jnp.exp(-jnp.abs(scores)))
+    failed = jnp.where(inside, -(jnp.maximum(scores, 0.0) + tail), 0.0)
+    blocks = [failed[:, b * 128 : (b + 1) * 128] for b in range(LEN // 128)]
+    later = (iota((128, 128), 0) > iota((128, 128), 1)).astype(F32)
+    within = jnp.dot(jnp.concatenate(blocks, axis=0), later, precision=HIGH, preferred_element_type=F32)
+    after = jnp.zeros((2 * ROWS, 1), F32)
+    sums = []
+    for b in reversed(range(LEN // 128)):
+        sums.insert(0, within[b * 32 : (b + 1) * 32] + after)
+        after = after + jnp.sum(blocks[b], axis=1, keepdims=True)
+    later_sum = jnp.concatenate(sums, axis=1)
+    weights = jnp.where(inside, jnp.exp(jnp.minimum(scores, 0.0) - tail + later_sum), 0.0).astype(BF16)
+    c_v.wait()
+    attended = jnp.zeros((2 * ROWS, HD), F32)
+    for p in range(ROWS // 2):
+        vals = jnp.concatenate([vbuf[2 * p], vbuf[2 * p + 1]], axis=1)
+        both = jnp.dot(weights, vals, preferred_element_type=F32)
+        attended = jnp.where(seq == 2 * p, both[:, 0:128], jnp.where(seq == 2 * p + 1, both[:, 128:256], attended))
+    norm = lax.rsqrt(jnp.mean(attended * attended, axis=1, keepdims=True) + EPSILON)
+    head = attended * norm * jnp.where(first, hgain[0:1], hgain[1:2])
+    hall[z] = jnp.concatenate([head[:ROWS], head[ROWS:]], axis=1).astype(BF16)
+
+    for d in (4, 3, 5, 2, 6, 1, 7):
+        send(hall.at[z], hall.at[z], h_sem.at[d - 1], at_z(d) * NX + x, t)
+    for d in (1, 2, 3):
+        arrived(wog.at[at_x(NX - d)], wo_sem.at[d - 1])
+    for d in (1, 7, 2, 6, 3, 5, 4):
+        arrived(hall.at[at_z(NZ - d)], h_sem.at[d - 1])
+    heads = hall[...].reshape(NZ * ROWS, 256)
+    for xi in range(NX):
+        part = jnp.dot(heads, wog[xi], preferred_element_type=F32)
+        obuf[:, :, xi * 128 : (xi + 1) * 128] = part.astype(BF16).reshape(NZ, ROWS, 128)
+    for d in (4, 5, 3, 2, 6, 7, 1):
+        send(obuf.at[at_t(d)], orecv.at[d - 1], o_sem.at[d - 1], e, at_t(d))
+    attn = obuf[t].astype(F32)
+    for d in (1, 7, 2, 6, 3, 5, 4):
+        arrived(orecv.at[d - 1], o_sem.at[d - 1])
+        attn = attn + orecv[d - 1].astype(F32)
+    attn = attn.astype(BF16)
+    for xi in range(NX):
+        abuf[xi] = attn[:, xi * 128 : (xi + 1) * 128]
+
+    for dt in range(NT):
+        for dx in range(NX):
+            if dt or dx:
+                send(abuf.at[at_x(dx)], agath.at[t, x], a_sem.at[dt * NX + dx], z * NX + at_x(dx), at_t(dt))
+    agath[t, x] = abuf[x]
+    for dt in range(NT):
+        for dx in range(NX):
+            if dt or dx:
+                arrived(agath.at[at_t(NT - dt), at_x(NX - dx)], a_sem.at[dt * NX + dx])
+    attn_out[...] = agath[...].reshape(512, 128)
+    for copy in started:
+        copy.wait_send()
+
+
+def front(stream, norm_gain, wq, wk, wv, boff, ck, cv, lens, wo, hgain):
+    any_spec = pl.BlockSpec(memory_space=pl.ANY)
+    vm = pl.BlockSpec(memory_space=pltpu.VMEM)
+    sm = pl.BlockSpec(memory_space=pltpu.SMEM)
+    dma = pltpu.SemaphoreType.DMA
+    return pl.pallas_call(
+        front_kernel,
+        name="front",
+        out_shape=(
+            jax.ShapeDtypeStruct((512, 128), BF16),
+            jax.ShapeDtypeStruct((16, 128), BF16),
+            jax.ShapeDtypeStruct((16, 128), BF16),
+        ),
+        in_specs=[any_spec] * 7 + [vm, vm, sm, sm],
+        out_specs=(vm, vm, vm),
+        scratch_shapes=[
+            pltpu.VMEM((NX, NZ, ROWS, 128), BF16),
+            pltpu.VMEM((128, 512), BF16),
+            pltpu.VMEM((ROWS, LEN, 128), BF16),
+            pltpu.VMEM((ROWS, LEN, 128), BF16),
+            pltpu.VMEM((NX, 128, 512), BF16),
+            pltpu.VMEM((NX - 1, 128, 512), BF16),
+            pltpu.VMEM((NX, 8, 128), F32),
+            pltpu.VMEM((NX - 1, 8, 128), F32),
+            pltpu.VMEM((NZ, ROWS, 512), BF16),
+            pltpu.VMEM((NZ - 1, ROWS, 512), BF16),
+            pltpu.VMEM((8, 128), F32),
+            pltpu.VMEM((NZ - 1, 8, 128), F32),
+            pltpu.VMEM((NX, 256, 128), BF16),
+            pltpu.VMEM((NZ, ROWS, 256), BF16),
+            pltpu.VMEM((NZ, ROWS, 512), BF16),
+            pltpu.VMEM((NT - 1, ROWS, 512), BF16),
+            pltpu.VMEM((NX, ROWS, 128), BF16),
+            pltpu.VMEM((NT, NX, ROWS, 128), BF16),
+            dma((16,)),
+            dma((96,)),
+            dma((3,)), dma((3,)), dma((3,)), dma((7,)), dma((7,)), dma((7,)), dma((7,)), dma((32,)),
+        ],
+        compiler_params=pltpu.CompilerParams(collective_id=0, has_side_effects=True, vmem_limit_bytes=60 * 1024 * 1024),
+    )(
+        stream.reshape(NZ, NX, ROWS, 128), wq, wk, wv, ck.reshape(ROWS, LEN, 128), cv.reshape(ROWS, LEN, 128), wo,
+        norm_gain.reshape(1, 128), hgain.reshape(2, 128), boff, lens,
+    )
 
 
 def sent_to_all(x, axis):
@@ -109,44 +346,10 @@
     model_width = stream.shape[1] * lax.axis_size("ep")
     block_width = stream.shape[1]
     seq_count = lengths.shape[0]
-    kv_local = cache_keys.shape[2]
-    head_dim = cache_keys.shape[3]
-    heads_local = break_offset.shape[0]
-    group_size = heads_local // kv_local
-    cache_len = cache_keys.shape[1]
     streamf = stream.astype(jnp.float32)
-    normed = rms_scale(streamf, norm_gain, model_width).astype(jnp.bfloat16)
-    projected = to_heads(normed, jnp.concatenate([w_query, w_key, w_value], axis=1))
-    q_width = w_query.shape[1]
-    k_width = w_key.shape[1]
-    queries = (
-        projected[:, :q_width]
-        .astype(jnp.bfloat16)
-        .reshape(seq_count, kv_local, group_size, head_dim)
-    )
-    key_rows = projected[:, q_width : q_width + k_width].astype(jnp.bfloat16)
-    value_rows = projected[:, q_width + k_width :].astype(jnp.bfloat16)
-    scores = jnp.einsum("skgd,slkd->skgl", queries, cache_keys, preferred_element_type=jnp.float32)
-    scores = (
-        scores * head_dim ** (-0.5) + break_offset.reshape(kv_local, group_size)[None, :, :, None]
-    )
-    in_cache = (jnp.arange(cache_len, dtype=jnp.int32)[None, :] < lengths[:, None])[
-        :, None, None, :
-    ]
-    failed = jnp.where(in_cache, jax.nn.log_sigmoid(-scores), 0.0)
-    later_sum = lax.cumsum(failed, axis=3, reverse=True) - failed
-    weights = jnp.where(in_cache, jnp.exp(jax.nn.log_sigmoid(scores) + later_sum), 0.0).astype(
-        jnp.bfloat16
-    )
-    attended = jnp.einsum(
-        "skgl,slkd->skgd", weights, cache_values, preferred_element_type=jnp.float32
-    )
-    gains = head_gain.reshape(kv_local, group_size, head_dim)[None]
-    normalized = (
-        attended * lax.rsqrt(jnp.mean(attended * attended, axis=3, keepdims=True) + EPSILON) * gains
-    )
-    head_out = normalized.astype(jnp.bfloat16).reshape(seq_count, heads_local * head_dim)
-    attn_out = from_heads(head_out, w_output)
+    attn_out, key_rows, value_rows = front(
+        stream, norm_gain, w_query, w_key, w_value, break_offset, cache_keys, cache_values, lengths, w_output, head_gain
+    )
     residual = streamf + attn_out.astype(jnp.float32)
     normed_ffn = rms_scale(residual, ffn_gain, model_width).astype(jnp.bfloat16)
     dense_width = dense_gate.shape[1]

time: 310 us -> 238 us (0.77)
  Pallas kernels: 0 us -> 44.6 us
  other arithmetic: 81 us -> 39.1 us
  waiting for transfers between devices: 72.8 us -> 40.6 us
  starting transfers between devices: 57.1 us -> 40.6 us
  blocking collectives: 48.7 us -> 33.3 us
  matrix products: 14.7 us -> 5.72 us
    pallas_call x0 -> x1, Pallas kernels: none -> 44.6 us  [front(): pl.pallas_call(front_kernel, name='front', out_shape=(jax.ShapeDtypeStruc...]
    another operation x5 -> x3, other arithmetic: 48.8 us -> 9.15 us
    all_to_all x1 -> x0, blocking collectives: 20.5 us -> none  [sent_to_all(): lax.all_to_all(jnp.broadcast_to(x[None], (size, *x.shape)), axis, 0, 0, t...]
    all_to_all x6 -> x4, waiting for transfers between devices: 43.3 us -> 25.3 us  [sent_to_all(): lax.all_to_all(jnp.broadcast_to(x[None], (size, *x.shape)), axis, 0, 0, t...]
    all_to_all x3 -> x2, waiting for transfers between devices: 22.1 us -> 7.97 us  [sent_and_summed(): lax.all_to_all(blocks, axis, split_axis=0, concat_axis=0, tiled=True)]
    all_to_all x6 -> x4, starting transfers between devices: 35.6 us -> 23.3 us  [sent_to_all(): lax.all_to_all(jnp.broadcast_to(x[None], (size, *x.shape)), axis, 0, 0, t...]
    dot_general x2 -> x0, matrix products: 6.71 us -> none  [the longest x1 3.41 us: per_device(): jnp.einsum('skgd,slkd->skgl', queries, cache_keys, preferred_element_type...]
    all_to_all x1, blocking collectives: 12 us -> 18 us  [per_device(): lax.all_to_all(own_slots, 'ep', split_axis=0, concat_axis=2, tiled=True)]
  transfers between devices with their start and end apart: 10 -> 7, of which waited for: 9 -> 5; matrix products, arithmetic and copies ran while one was open for 20% -> 26% of each run, Pallas kernels for 0% -> 0%
where the time goes in v1:
time: 238 us; the launch traced here: 237 us
  Pallas kernels  44.6 us (19%)
  starting transfers between devices  40.6 us (17%)
  waiting for transfers between devices  40.6 us (17%)
  other arithmetic  39.1 us (16%)
  blocking collectives  33.3 us (14%)
  local copies, waits for them, and re-layouts  31.8 us (13%)
  matrix products  5.72 us (2%)
    pallas_call x1, Pallas kernels, front(): pl.pallas_call(front_kernel, name='front', out_shape=(jax.ShapeDtypeStruc...  44.6 us
    all_to_all x4, waiting for transfers between devices, sent_to_all(): lax.all_to_all(jnp.broadcast_to(x[None], (size, *x.shape)), axis, 0, 0, t...  25.3 us
    unnamed x1, other arithmetic  23.4 us
    all_to_all x4, starting transfers between devices, sent_to_all(): lax.all_to_all(jnp.broadcast_to(x[None], (size, *x.shape)), axis, 0, 0, t...  23.3 us
    all_to_all x1, blocking collectives, per_device(): lax.all_to_all(own_slots, 'ep', split_axis=0, concat_axis=2, tiled=True)  18 us
    all_gather x1, blocking collectives, per_device(): gathered = lax.all_gather(arrived, 'tp', axis=1, tiled=True)  15.3 us
    another operation x3, other arithmetic  9.15 us
    all_to_all x1, starting transfers between devices, per_device(): lax.all_to_all(summed, 'ep', split_axis=2, concat_axis=0, tiled=True)  8.97 us
  transfers between devices with their start and end apart: 7, of which 5 were waited for; matrix products, arithmetic and copies ran while one was open for 26% of the time, Pallas kernels for 0%

profile of v1, /device:TPU:1, one launch (start us, length us, event | category | flops | bytes accessed | tf_op | source)
XLA Modules:
  0.0 236.8 jit_solution(6101161294276287359)
XLA Ops:
  0.7 44.6 %front.1 = (bf16[512,128]{1,0:T(8,128)(2,1)}, bf16[16,128]{1,0:T(8,128)(2,1)}, bf16[16,128]{1,0:T(8,128)(2,1)}) custom-call(bf16[8,4,16,128]{3,2,1,0:T(8,128)(2,1)} %bitcast.79, bf16[128,256]{1,0:T(8,128)(2,1)} %wq.1, bf16[128,128]{1,0:T(8,128)(2,1)} %wk.1, bf16[128,128]{1,0:T(8,128)(2,1)} %wv.1, bf16[16,1024,128]{2,1,0:T(8,128)(2,1)} %bitcast.77, ...), custom_call_target="tpu_custom_call" | custom-call | tf_op jit(solution)/shard_map/front/pallas_call | solution.py:206
  45.3 1.1 multiply_reduce_fusion
  47.1 6.0 %all-to-all-start = ((f32[32,1,512]{2,1,0:T(1,128)}), f32[32,1,512]{2,1,0:T(1,128)S(1)}, u32[]{:S(2)}, u32[]{:S(2)}) async-start(f32[32,1,512]{2,1,0:T(1,128)} %broadcast_in_dim.14), calls=%async_computation | async-start | bytes 131072 | tf_op jit(solution)/shard_map/all_to_all | solution.py:248
  53.7 9.0 %reduce-window.6 = s32[32,8,128]{2,1,0:T(8,128)S(1)} reduce-window(s32[32,8,128]{2,1,0:T(8,128)S(1)} %fusion.17, s32[]{:T(128)} %constant.46.clone.1), window={size=1x1x128 pad=0_0x0_0x127_0}, to_apply=%region_2.0 | reduce-window | flops 4161536 | bytes 262148 | tf_op jit(solution)/shard_map/reduce-window
  63.5 4.3 %scatter_custom_fusion = s32[2048]{0:T(1024)S(1)} fusion(s32[1024]{0:T(1024)S(1)} %bitcast.90, s32[1024]{0:T(1024)S(1)} %add_select_fusion, s32[]{:T(128)} %constant.44.clone.1), kind=kCustom, calls=%fused_computation.51 | custom fusion | bytes 8196 | tf_op jit(solution)/shard_map/scatter | solution.py:318
  68.1 6.2 %gather_fusion = bf16[2048,128]{1,0:T(8,128)(2,1)S(1)} fusion(bf16[513,128]{1,0:T(8,128)(2,1)S(1)} %concatenate.6, s32[2048]{0:T(1024)S(1)} %fusion.25), kind=kCustom, calls=%fused_computation | custom fusion | bytes 1056768 | tf_op jit(solution)/shard_map/gather | solution.py:365
  74.4 18.0 %all_to_all.64 = bf16[32,8,128]{2,1,0:T(8,128)(2,1)S(1)} all-to-all(bf16[32,8,128]{2,1,0:T(8,128)(2,1)S(1)} %constant_dynamic-slice_fusion), channel_id=1, replica_groups=mesh['ep'=32,'tp'=8] {'ep'}, dimensions={0} | all-to-all | bytes 131072 | tf_op jit(solution)/shard_map/all_to_all | solution.py:368
  92.4 15.3 %all_gather.3 = bf16[1,64,4096]{2,1,0:T(8,128)(2,1)S(1)} all-gather(bf16[1,8,4096]{2,1,0:T(8,128)(2,1)S(1)} %bitcast.84), channel_id=1, replica_groups=mesh['ep'=32,'tp'=8] {'tp'}, dimensions={1}, use_global_device_ids=true | all-gather | bytes 589824 | tf_op jit(solution)/shard_map/all_gather | solution.py:369
  107.7 1.5 fusion.5
  109.3 1.4 fusion
  110.7 3.6 %all-to-all-start.2 = ((bf16[8,1,8,4096]{3,2,1,0:T(8,128)(2,1)}), bf16[8,1,8,4096]{3,2,1,0:T(8,128)(2,1)S(1)}, u32[]{:S(2)}, u32[]{:S(2)}) async-start(bf16[8,1,8,4096]{3,2,1,0:T(8,128)(2,1)} %fusion), calls=%async_computation.2 | async-start | bytes 1048576 | tf_op jit(solution)/shard_map/all_to_all | solution.py:263
  114.2 1.4 convolution_convert_fusion.1
  115.6 8.0 %all-to-all-done.2 = bf16[8,1,8,4096]{3,2,1,0:T(8,128)(2,1)S(1)} async-done(((bf16[8,1,8,4096]{3,2,1,0:T(8,128)(2,1)}), bf16[8,1,8,4096]{3,2,1,0:T(8,128)(2,1)S(1)}, u32[]{:S(2)}, u32[]{:S(2)}) %all-to-all-start.2) | async-done | bytes 524320 | tf_op jit(solution)/shard_map/all_to_all | solution.py:263
  123.6 4.8 %all-to-all-start.5 = ((bf16[32,16,1024]{2,1,0:T(8,128)(2,1)}), bf16[32,16,1024]{2,1,0:T(8,128)(2,1)}, u32[]{:S(2)}, u32[]{:S(2)}) async-start(bf16[32,16,1024]{2,1,0:T(8,128)(2,1)} %bitcast.25), calls=%async_computation.5 | async-start | bytes 2097152 | tf_op jit(solution)/shard_map/all_to_all | solution.py:263
  128.5 2.8 %copy.69 = bf16[1,8,4096]{1,0,2:T(2,128)(2,1)S(1)} copy(bf16[1,8,4096]{2,1,0:T(8,128)(2,1)S(1)} %bitcast.87) | data formatting | bytes 131072 | tf_op jit(solution)/shard_map/reduce_sum | solution.py:264
  131.8 23.4 %reduce.4 = bf16[4096,8]{1,0:T(8,128)(2,1)} reduce(bf16[4096,1,8]{2,1,0:T(2,128)(2,1)S(1)} %bitcast.75, bf16[]{:T(256)} %broadcast.96), dimensions={1}, to_apply=%bitcast.67.reduce_sub_computation | reduce | bytes 131074
  155.2 3.1 %reshape.167 = bf16[32,2,512]{2,1,0:T(2,128)(2,1)} reshape(bf16[4096,8]{1,0:T(8,128)(2,1)} %reduce.4) | data formatting | bytes 131072
  158.3 9.0 %all-to-all-start.3 = ((bf16[32,2,512]{2,1,0:T(2,128)(2,1)}), bf16[32,2,512]{2,1,0:T(2,128)(2,1)S(1)}, u32[]{:S(2)}, u32[]{:S(2)}) async-start(bf16[32,2,512]{2,1,0:T(2,128)(2,1)} %reshape.167), calls=%async_computation.3 | async-start | bytes 131072 | tf_op jit(solution)/shard_map/all_to_all | solution.py:372
  167.3 1.4 convert_reduce_fusion
  168.7 7.4 %all-to-all-done.3 = bf16[32,2,512]{2,1,0:T(2,128)(2,1)S(1)} async-done(((bf16[32,2,512]{2,1,0:T(2,128)(2,1)}), bf16[32,2,512]{2,1,0:T(2,128)(2,1)S(1)}, u32[]{:S(2)}, u32[]{:S(2)}) %all-to-all-start.3) | async-done | bytes 65568 | tf_op jit(solution)/shard_map/all_to_all | solution.py:372
  177.0 4.6 %all-to-all-start.6 = ((bf16[32,16,512]{2,1,0:T(8,128)(2,1)}), bf16[32,16,512]{2,1,0:T(8,128)(2,1)}, u32[]{:S(2)}, u32[]{:S(2)}) async-start(bf16[32,16,512]{2,1,0:T(8,128)(2,1)} %broadcast_in_dim.19), calls=%async_computation.6 | async-start | bytes 1048576 | tf_op jit(solution)/shard_map/all_to_all | solution.py:248
  181.6 2.8 %reshape.168 = bf16[4096,1,8]{2,1,0:T(2,128)(2,1)S(1)} reshape(bf16[32,2,512]{2,1,0:T(2,128)(2,1)S(1)} %all-to-all-done.3) | data formatting | bytes 131072
  184.4 1.9 copy.70
  186.3 9.4 %all-to-all-done.6 = bf16[32,16,512]{2,1,0:T(8,128)(2,1)} async-done(((bf16[32,16,512]{2,1,0:T(8,128)(2,1)}), bf16[32,16,512]{2,1,0:T(8,128)(2,1)}, u32[]{:S(2)}, u32[]{:S(2)}) %all-to-all-start.6) | async-done | bytes 524320 | tf_op jit(solution)/shard_map/all_to_all | solution.py:248
  196.6 8.2 %all-to-all-start.4 = ((bf16[8,32,8,128]{3,2,1,0:T(8,128)(2,1)}), bf16[8,32,8,128]{3,2,1,0:T(8,128)(2,1)S(1)}, u32[]{:S(2)}, u32[]{:S(2)}) async-start(bf16[8,32,8,128]{3,2,1,0:T(8,128)(2,1)} %broadcast_in_dim.18), calls=%async_computation.4 | async-start | bytes 1048576 | tf_op jit(solution)/shard_map/all_to_all | solution.py:248
  204.8 1.4 convolution_convert_fusion.2
  206.2 8.0 %all-to-all-done.4 = bf16[8,32,8,128]{3,2,1,0:T(8,128)(2,1)S(1)} async-done(((bf16[8,32,8,128]{3,2,1,0:T(8,128)(2,1)}), bf16[8,32,8,128]{3,2,1,0:T(8,128)(2,1)S(1)}, u32[]{:S(2)}, u32[]{:S(2)}) %all-to-all-start.4) | async-done | bytes 524320 | tf_op jit(solution)/shard_map/all_to_all | solution.py:248
  214.2 1.1 broadcast_in_dim.20
  215.3 4.4 %all-to-all-start.7 = ((bf16[8,512,128]{2,1,0:T(8,128)(2,1)}), bf16[8,512,128]{2,1,0:T(8,128)(2,1)S(1)}, u32[]{:S(2)}, u32[]{:S(2)}) async-start(bf16[8,512,128]{2,1,0:T(8,128)(2,1)} %broadcast_in_dim.20), calls=%async_computation.7 | async-start | bytes 2097152 | tf_op jit(solution)/shard_map/all_to_all | solution.py:248
  220.9 3.2 %gather_fusion.1 = bf16[1024,128]{1,0:T(8,128)(2,1)S(1)} fusion(bf16[2048,128]{1,0:T(8,128)(2,1)S(1)} %bitcast.74, s32[1024]{0:T(1024)S(1)} %broadcast_clamp_fusion), kind=kCustom, calls=%fused_computation.1 | custom fusion | bytes 528384 | tf_op jit(solution)/shard_map/gather | solution.py:374
  224.1 2.8 %fusion.7 = f32[512,128]{1,0:T(8,128)S(1)} fusion(bf16[512,2,128]{2,1,0:T(2,128)(2,1)S(1)} %bitcast.81, f32[512,2]{1,0:T(8,128)S(1)} %copy-done.4), kind=kLoop, calls=%fused_computation.15 | loop fusion | flops 327680 | bytes 528384 | tf_op jit(solution)/shard_map/reduce_sum | solution.py:379
  226.9 7.9 %all-to-all-done.7 = bf16[8,512,128]{2,1,0:T(8,128)(2,1)S(1)} async-done(((bf16[8,512,128]{2,1,0:T(8,128)(2,1)}), bf16[8,512,128]{2,1,0:T(8,128)(2,1)S(1)}, u32[]{:S(2)}, u32[]{:S(2)}) %all-to-all-start.7) | async-done | bytes 1048608 | tf_op jit(solution)/shard_map/all_to_all | solution.py:248
  (67 shorter events, 7.8 us)
Async XLA Ops:
  0.6 108.6 %copy-start = (bf16[1,128,4096]{2,1,0:T(8,128)(2,1)S(1)}, bf16[1,128,4096]{2,1,0:T(8,128)(2,1)}, u32[]{:S(2)}) copy-start(bf16[1,128,4096]{2,1,0:T(8,128)(2,1)} %param.37) | copy-start | bytes 3145732
  0.7 44.7 %copy-start.1 = (bf16[512,128]{1,0:T(8,128)(2,1)S(1)}, bf16[512,128]{1,0:T(8,128)(2,1)}, u32[]{:S(2)}) copy-start(bf16[512,128]{1,0:T(8,128)(2,1)} %param.21) | copy-start | bytes 393220
  0.7 52.5 %copy-start.7 = (s32[512,2]{0,1:T(2,128)S(1)}, s32[512,2]{0,1:T(2,128)}, u32[]{:S(2)}) copy-start(s32[512,2]{0,1:T(2,128)} %param.33) | copy-start | bytes 12292
  45.3 22.7 %copy-start.2 = (bf16[512,128]{1,0:T(8,128)(2,1)S(1)}, bf16[512,128]{1,0:T(8,128)(2,1)}, u32[]{:S(2)}) copy-start(bf16[512,128]{1,0:T(8,128)(2,1)} %get-tuple-element.6) | copy-start | bytes 393220
  45.3 22.7 %copy-start.11 = (f32[128]{0:T(128)S(1)}, f32[128]{0:T(128)}, u32[]{:S(2)}) copy-start(f32[128]{0:T(128)} %param.32) | copy-start | bytes 1540
  47.1 20.8 %all-to-all-start = ((f32[32,1,512]{2,1,0:T(1,128)}), f32[32,1,512]{2,1,0:T(1,128)S(1)}, u32[]{:S(2)}, u32[]{:S(2)}) async-start(f32[32,1,512]{2,1,0:T(1,128)} %broadcast_in_dim.14), calls=%async_computation | async-start | bytes 131072 | tf_op jit(solution)/shard_map/all_to_all | solution.py:248
  74.3 34.9 %copy-start.3 = (bf16[1,4096,128]{2,1,0:T(8,128)(2,1)S(1)}, bf16[1,4096,128]{2,1,0:T(8,128)(2,1)}, u32[]{:S(2)}) copy-start(bf16[1,4096,128]{2,1,0:T(8,128)(2,1)} %param.36) | copy-start | bytes 3145732
  109.2 5.0 %copy-start.5 = (bf16[128,512]{1,0:T(8,128)(2,1)S(1)}, bf16[128,512]{1,0:T(8,128)(2,1)}, u32[]{:S(2)}) copy-start(bf16[128,512]{1,0:T(8,128)(2,1)} %param.39) | copy-start | bytes 393220
  109.2 5.0 %copy-start.6 = (bf16[128,512]{1,0:T(8,128)(2,1)S(1)}, bf16[128,512]{1,0:T(8,128)(2,1)}, u32[]{:S(2)}) copy-start(bf16[128,512]{1,0:T(8,128)(2,1)} %param.38) | copy-start | bytes 393220
  110.7 12.9 %all-to-all-start.2 = ((bf16[8,1,8,4096]{3,2,1,0:T(8,128)(2,1)}), bf16[8,1,8,4096]{3,2,1,0:T(8,128)(2,1)S(1)}, u32[]{:S(2)}, u32[]{:S(2)}) async-start(bf16[8,1,8,4096]{3,2,1,0:T(8,128)(2,1)} %fusion), calls=%async_computation.2 | async-start | bytes 1048576 | tf_op jit(solution)/shard_map/all_to_all | solution.py:263
  123.6 34.7 %all-to-all-start.5 = ((bf16[32,16,1024]{2,1,0:T(8,128)(2,1)}), bf16[32,16,1024]{2,1,0:T(8,128)(2,1)}, u32[]{:S(2)}, u32[]{:S(2)}) async-start(bf16[32,16,1024]{2,1,0:T(8,128)(2,1)} %bitcast.25), calls=%async_computation.5 | async-start | bytes 2097152 | tf_op jit(solution)/shard_map/all_to_all | solution.py:263
  158.3 17.8 %all-to-all-start.3 = ((bf16[32,2,512]{2,1,0:T(2,128)(2,1)}), bf16[32,2,512]{2,1,0:T(2,128)(2,1)S(1)}, u32[]{:S(2)}, u32[]{:S(2)}) async-start(bf16[32,2,512]{2,1,0:T(2,128)(2,1)} %reshape.167), calls=%async_computation.3 | async-start | bytes 131072 | tf_op jit(solution)/shard_map/all_to_all | solution.py:372
  177.0 18.8 %all-to-all-start.6 = ((bf16[32,16,512]{2,1,0:T(8,128)(2,1)}), bf16[32,16,512]{2,1,0:T(8,128)(2,1)}, u32[]{:S(2)}, u32[]{:S(2)}) async-start(bf16[32,16,512]{2,1,0:T(8,128)(2,1)} %broadcast_in_dim.19), calls=%async_computation.6 | async-start | bytes 1048576 | tf_op jit(solution)/shard_map/all_to_all | solution.py:248
  196.6 17.6 %all-to-all-start.4 = ((bf16[8,32,8,128]{3,2,1,0:T(8,128)(2,1)}), bf16[8,32,8,128]{3,2,1,0:T(8,128)(2,1)S(1)}, u32[]{:S(2)}, u32[]{:S(2)}) async-start(bf16[8,32,8,128]{3,2,1,0:T(8,128)(2,1)} %broadcast_in_dim.18), calls=%async_computation.4 | async-start | bytes 1048576 | tf_op jit(solution)/shard_map/all_to_all | solution.py:248
  204.8 14.9 %copy-start.8 = (f32[512,2]{0,1:T(2,128)S(1)}, f32[512,2]{0,1:T(2,128)}, u32[]{:S(2)}) copy-start(f32[512,2]{0,1:T(2,128)} %param.34) | copy-start | bytes 12292
  215.3 19.4 %all-to-all-start.7 = ((bf16[8,512,128]{2,1,0:T(8,128)(2,1)}), bf16[8,512,128]{2,1,0:T(8,128)(2,1)S(1)}, u32[]{:S(2)}, u32[]{:S(2)}) async-start(bf16[8,512,128]{2,1,0:T(8,128)(2,1)} %broadcast_in_dim.20), calls=%async_computation.7 | async-start | bytes 2097152 | tf_op jit(solution)/shard_map/all_to_all | solution.py:248
  220.8 3.3 %copy-start.4 = (f32[512,2]{1,0:T(8,128)S(1)}, f32[512,2]{1,0:T(8,128)}, u32[]{:S(2)}) copy-start(f32[512,2]{1,0:T(8,128)} %copy.73) | copy-start | bytes 12292
  220.8 14.1 %copy-start.12 = (f32[128]{0:T(128)S(1)}, f32[128]{0:T(128)}, u32[]{:S(2)}) copy-start(f32[128]{0:T(128)} %param.41) | copy-start | bytes 1540
  220.8 14.8 %copy-start.10 = (bf16[16,128]{1,0:T(8,128)(2,1)S(1)}, bf16[16,128]{1,0:T(8,128)(2,1)}, u32[]{:S(2)}) copy-start(bf16[16,128]{1,0:T(8,128)(2,1)} %get-tuple-element.13) | copy-start | bytes 12292
  220.8 15.4 %copy-start.9 = (bf16[16,128]{1,0:T(8,128)(2,1)S(1)}, bf16[16,128]{1,0:T(8,128)(2,1)}, u32[]{:S(2)}) copy-start(bf16[16,128]{1,0:T(8,128)(2,1)} %get-tuple-element.14) | copy-start | bytes 12292

commit v2 on v1

v2 whole, which is shorter than its diff:
```python
import jax
import jax.numpy as jnp
from jax import lax
from jax.experimental import pallas as pl
from jax.experimental.pallas import tpu as pltpu
from jax.sharding import PartitionSpec as P

EPSILON = 1e-06
NX, NZ, NT = 4, 8, 8
MODEL, HD, LEN, ROWS, SEQS = 4096, 128, 1024, 16, 512
CAP, HALF = 64, 32
F32, BF16 = jnp.float32, jnp.bfloat16
HIGH = lax.Precision.HIGHEST
MESH = pl.DeviceIdType.MESH
FAR_FIRST = (4, 3, 5, 2, 6, 1, 7)
NEAR_FIRST = (1, 7, 2, 6, 3, 5, 4)


def iota(shape, dim):
    return lax.broadcasted_iota(jnp.int32, shape, dim)


def step_kernel(
    stream, wq, wk, wv, ck, cv, wo, eg, eu, ed, dg, du, dd,
    ngain, hgain, fgain, mgain, route, rweights, boff, lens,
    mixed, key_rows, value_rows,
    strm, wqkv, kbuf, vbuf, ybuf, yrecv, ssq, ssqr, zbuf, zrecv, zsq, zsqr,
    wog, hall, obuf, orecv, abuf, afin, sres, fgb, fgall, wgu, ddb, egb, eub, edb,
    pmat, ctm, rbuf, rall, gbuf, fsq, fsqr, gub, gurecv, dbuf, xe, hd,
    pown, pout, precv, rsum, rt, fbuf, frecv, mgath,
    lsem, ssem,
    yx_sem, sx_sem, wo_sem, wg_sem, wu_sem, sr_sem, fg_sem, yz_sem, sz_sem, h_sem, o_sem, af_sem, r_sem,
    fs_sem, gu_sem, d_sem, xe_sem, hz_sem, hx_sem, p_sem, rt_sem, f_sem, m_sem,
):
    e = lax.axis_index("ep")
    t = lax.axis_index("tp")
    z = lax.div(e, NX)
    x = lax.rem(e, NX)
    c = lax.rem(t, 2)
    partner = t + 1 - 2 * c

    def at_x(d):
        return lax.rem(x + d, NX)

    def at_z(d):
        return lax.rem(z + d, NZ)

    def at_t(d):
        return lax.rem(t + d, NT)

    started = []

    def send(src, dst, rsem, dev_e, dev_t):
        copy = pltpu.make_async_remote_copy(
            src_ref=src, dst_ref=dst, send_sem=ssem.at[len(started)], recv_sem=rsem,
            device_id=(dev_e, dev_t), device_id_type=MESH,
        )
        copy.start()
        started.append(copy)

    def arrived(dst, rsem):
        pltpu.make_async_copy(dst, dst, rsem).wait()

    loads = []

    def load(src, dst):
        copy = pltpu.make_async_copy(src, dst, lsem.at[len(loads)])
        copy.start()
        loads.append(copy)
        return copy

    def columns(ref, block):
        return ref.at[:, pl.ds(pl.multiple_of(block * 128, 128), 128)]

    c_w = [load(wq, wqkv.at[:, 0:256]), load(wk, wqkv.at[:, 256:384]), load(wv, wqkv.at[:, 384:512])]
    c_s = [load(stream.at[:, xi], strm.at[xi]) for xi in range(NX)]

    barrier = pltpu.get_barrier_semaphore()
    peers = 0
    for dt in range(NT):
        for dz in range(NZ):
            for dx in range(NX):
                if (dt == 0 and (dz or dx)) or (dt and dz == 0):
                    pl.semaphore_signal(barrier, inc=1, device_id=(at_z(dz) * NX + at_x(dx), at_t(dt)), device_id_type=MESH)
                    peers += 1

    c_wo = load(wo, wog.at[x])
    c_k = load(ck, kbuf)
    c_v = load(cv, vbuf)
    c_dg = load(columns(dg, x), wgu.at[x, :, 0:128])
    c_du = load(columns(du, x), wgu.at[x, :, 128:256])
    c_dd = load(dd, ddb)
    c_eg = load(eg, egb)
    c_eu = load(eu, eub)
    c_ed = [load(ed.at[:, zi * 512 : (zi + 1) * 512], edb.at[zi]) for zi in range(NZ)]

    for copy in c_w + c_s:
        copy.wait()
    gain = ngain[...]
    w = wqkv[...]
    for xi in range(NX):
        rows = strm[xi].reshape(NZ * ROWS, HD).astype(F32)
        ybuf[xi] = jnp.dot((rows * gain).astype(BF16), w, preferred_element_type=F32).astype(BF16)
        sums = jnp.sum((rows * rows).T, axis=0, keepdims=True)
        ssq[xi] = jnp.broadcast_to(sums, (8, HD))
    fgb[...] = jnp.broadcast_to(fgain[...], (8, HD))

    pl.semaphore_wait(barrier, peers)

    for d in (2, 1, 3):
        to = z * NX + at_x(d)
        send(ybuf.at[at_x(d)], yrecv.at[d - 1], yx_sem.at[d - 1], to, t)
        send(ssq.at[at_x(d)], ssqr.at[d - 1], sx_sem.at[d - 1], to, t)
    c_wo.wait()
    for d in (2, 1, 3):
        to = z * NX + at_x(d)
        send(wog.at[x], wog.at[x], wo_sem.at[d - 1], to, t)
        send(strm.at[at_x(d), t], sres.at[x], sr_sem.at[d - 1], to, t)
        send(fgb, fgall.at[x], fg_sem.at[d - 1], to, t)
        send(columns(dg, at_x(d)), wgu.at[x, :, 0:128], wg_sem.at[d - 1], to, t)
        send(columns(du, at_x(d)), wgu.at[x, :, 128:256], wu_sem.at[d - 1], to, t)
    sres[x] = strm[x, t]
    fgall[x] = fgb[...]

    names = [route[0:1], route[1:2]]
    expert = iota((32, SEQS), 0)
    chosen = (jnp.where(names[0] == expert, 1.0, 0.0) + jnp.where(names[1] == expert, 1.0, 0.0)).astype(BF16)
    before = jnp.where(iota((SEQS, SEQS), 0) < iota((SEQS, SEQS), 1), 1.0, 0.0).astype(BF16)
    earlier = jnp.dot(chosen, before, preferred_element_type=F32)
    slots = [
        n * CAP + jnp.sum(jnp.where(n == expert, earlier, 0.0), axis=0, keepdims=True).astype(jnp.int32) for n in names
    ]
    weight_sum = rweights[0:1] + rweights[1:2]
    shares = [rweights[0:1] / weight_sum, rweights[1:2] / weight_sum]
    for i in range(2):
        row = iota((128, SEQS), 0) + i * 128
        slot = lax.shift_right_logical(row, 5) * (NX * CAP) + (x * CAP + c * HALF) + (row & 31)
        pmat[i * 128 : (i + 1) * 128] = jnp.where((slots[0] == slot) | (slots[1] == slot), 1.0, 0.0).astype(BF16)
    for i in range(8):
        row = iota((128, SEQS), 0) + i * 128
        slot = lax.shift_right_logical(row, 5) * CAP + c * HALF + (row & 31)
        ctm[i * 128 : (i + 1) * 128] = jnp.where(
            slots[0] == slot, shares[0], jnp.where(slots[1] == slot, shares[1], 0.0)
        ).astype(BF16)

    total = ybuf[x].astype(F32)
    sq = ssq[x]
    for d in (1, 3, 2):
        arrived(yrecv.at[d - 1], yx_sem.at[d - 1])
        arrived(ssqr.at[d - 1], sx_sem.at[d - 1])
        total = total + yrecv[d - 1].astype(F32)
        sq = sq + ssqr[d - 1]
    zbuf[...] = total.astype(BF16).reshape(NZ, ROWS, 512)
    zsq[...] = sq

    for d in FAR_FIRST:
        to = at_z(d) * NX + x
        send(zbuf.at[at_z(d)], zrecv.at[d - 1], yz_sem.at[d - 1], to, t)
        send(zsq, zsqr.at[d - 1], sz_sem.at[d - 1], to, t)
    qkv = zbuf[z].astype(F32)
    sq = zsq[...]
    for d in NEAR_FIRST:
        arrived(zrecv.at[d - 1], yz_sem.at[d - 1])
        arrived(zsqr.at[d - 1], sz_sem.at[d - 1])
        qkv = qkv + zrecv[d - 1].astype(F32)
        sq = sq + zsqr[d - 1]
    lane = iota((ROWS, HD), 1)
    pick = lane == z * ROWS + iota((ROWS, HD), 0)
    mean = jnp.sum(jnp.where(pick, jnp.broadcast_to(sq[0:1], (ROWS, HD)), 0.0), axis=1, keepdims=True) / MODEL
    qkv = qkv * lax.rsqrt(mean + EPSILON)
    key_rows[...] = qkv[:, 256:384].astype(BF16)
    value_rows[...] = qkv[:, 384:512].astype(BF16)

    q = jnp.concatenate([qkv[:, 0:128], qkv[:, 128:256]], axis=0).astype(BF16).astype(F32)
    seq = lax.rem(iota((2 * ROWS, 1), 0), ROWS)
    c_k.wait()
    scores = jnp.zeros((2 * ROWS, LEN), F32)
    for p in range(ROWS // 2):
        keys = jnp.concatenate([kbuf[2 * p], kbuf[2 * p + 1]], axis=1)
        own = jnp.concatenate([jnp.where(seq == 2 * p, q, 0.0), jnp.where(seq == 2 * p + 1, q, 0.0)], axis=1)
        scores = scores + lax.dot_general(own.astype(BF16), keys, (((1,), (1,)), ((), ())), preferred_element_type=F32)
    first = iota((2 * ROWS, 1), 0) < ROWS
    length = jnp.zeros((2 * ROWS, 1), jnp.int32)
    for s in range(ROWS):
        length = jnp.where(seq == s, lens[s], length)
    scores = scores * HD ** (-0.5) + jnp.where(first, boff[0], boff[1])
    inside = iota((2 * ROWS, LEN), 1) < length
    tail = jnp.log1p(jnp.exp(-jnp.abs(scores)))
    failed = jnp.where(inside, -(jnp.maximum(scores, 0.0) + tail), 0.0)
    blocks = [failed[:, b * 128 : (b + 1) * 128] for b in range(LEN // 128)]
    later = (iota((128, 128), 0) > iota((128, 128), 1)).astype(F32)
    within = jnp.dot(jnp.concatenate(blocks, axis=0), later, precision=HIGH, preferred_element_type=F32)
    after = jnp.zeros((2 * ROWS, 1), F32)
    sums = []
    for b in reversed(range(LEN // 128)):
        sums.insert(0, within[b * 32 : (b + 1) * 32] + after)
        after = after + jnp.sum(blocks[b], axis=1, keepdims=True)
    later_sum = jnp.concatenate(sums, axis=1)
    weights = jnp.where(inside, jnp.exp(jnp.minimum(scores, 0.0) - tail + later_sum), 0.0).astype(BF16)
    c_v.wait()
    attended = jnp.zeros((2 * ROWS, HD), F32)
    for p in range(ROWS // 2):
        vals = jnp.concatenate([vbuf[2 * p], vbuf[2 * p + 1]], axis=1)
        both = jnp.dot(weights, vals, preferred_element_type=F32)
        attended = jnp.where(seq == 2 * p, both[:, 0:128], jnp.where(seq == 2 * p + 1, both[:, 128:256], attended))
    norm = lax.rsqrt(jnp.mean(attended * attended, axis=1, keepdims=True) + EPSILON)
    head = attended * norm * jnp.where(first, hgain[0:1], hgain[1:2])
    hall[z] = jnp.concatenate([head[:ROWS], head[ROWS:]], axis=1).astype(BF16)

    for d in FAR_FIRST:
        send(hall.at[z], hall.at[z], h_sem.at[d - 1], at_z(d) * NX + x, t)
    for d in (1, 2, 3):
        arrived(wog.at[at_x(NX - d)], wo_sem.at[d - 1])
        arrived(sres.at[at_x(NX - d)], sr_sem.at[d - 1])
        arrived(fgall.at[at_x(NX - d)], fg_sem.at[d - 1])
        arrived(wgu.at[at_x(NX - d), :, 0:128], wg_sem.at[d - 1])
        arrived(wgu.at[at_x(NX - d), :, 128:256], wu_sem.at[d - 1])
    c_dg.wait()
    c_du.wait()
    for d in NEAR_FIRST:
        arrived(hall.at[at_z(NZ - d)], h_sem.at[d - 1])
    heads = hall[...].reshape(NZ * ROWS, 256)
    for xi in range(NX):
        part = jnp.dot(heads, wog[xi], preferred_element_type=F32)
        obuf[:, :, xi * 128 : (xi + 1) * 128] = part.astype(BF16).reshape(NZ, ROWS, 128)
    for d in (4, 5, 3, 2, 6, 7, 1):
        send(obuf.at[at_t(d)], orecv.at[d - 1], o_sem.at[d - 1], e, at_t(d))
    attn = obuf[t].astype(F32)
    for d in NEAR_FIRST:
        arrived(orecv.at[d - 1], o_sem.at[d - 1])
        attn = attn + orecv[d - 1].astype(F32)
    attn = attn.astype(BF16)
    rbuf[...] = (attn.astype(F32) + jnp.concatenate([sres[xi].astype(F32) for xi in range(NX)], axis=1)).astype(BF16)
    for xi in range(NX):
        abuf[xi] = attn[:, xi * 128 : (xi + 1) * 128]

    for dt in (4, 5, 3, 2, 6, 7, 1, 0):
        for dx in (2, 1, 3, 0):
            if dt or dx:
                send(rbuf, rall.at[t, x], r_sem.at[dt * NX + dx], z * NX + at_x(dx), at_t(dt))
    for d in (2, 1, 3):
        send(abuf.at[at_x(d)], afin.at[x], af_sem.at[d - 1], z * NX + at_x(d), t)
    rall[t, x] = rbuf[...]
    afin[x] = abuf[x]
    for dt in range(NT):
        for dx in range(NX):
            if dt or dx:
                arrived(rall.at[at_t(NT - dt), at_x(NX - dx)], r_sem.at[dt * NX + dx])
    gains = jnp.concatenate([fgall[xi][0:1] for xi in range(NX)], axis=1)
    square_rows = []
    for i in range(4):
        rows = rall[2 * i : 2 * i + 2].reshape(128, 512).astype(F32)
        gbuf[i * 128 : (i + 1) * 128] = (rows * gains).astype(BF16)
        squares = rows * rows
        squares = squares[:, 0:128] + squares[:, 128:256] + squares[:, 256:384] + squares[:, 384:512]
        square_rows.append(jnp.sum(squares.T, axis=0, keepdims=True))
    fsq[...] = jnp.concatenate(square_rows + [jnp.zeros((4, 128), F32)], axis=0)
    dispatched = jnp.dot(pmat[...], gbuf[...], preferred_element_type=F32)
    dbuf[...] = dispatched.astype(BF16).reshape(NZ, HALF, 512)
    for d in FAR_FIRST:
        to = at_z(d) * NX + x
        send(dbuf.at[at_z(d)], xe.at[c, z], d_sem.at[d - 1], to, t)
        send(fsq, fsqr.at[d - 1], fs_sem.at[d - 1], to, t)
    xe[c, z] = dbuf[z]
    wide = wgu[...].reshape(512, 256)
    for i in range(4):
        part = jnp.dot(gbuf[i * 128 : (i + 1) * 128], wide, preferred_element_type=F32)
        gub[2 * i : 2 * i + 2] = part.astype(BF16).reshape(2, 64, 256)
    for d in FAR_FIRST:
        send(gub.at[at_z(d)], gurecv.at[d - 1], gu_sem.at[d - 1], at_z(d) * NX + x, t)

    send(xe.at[c, z], xe.at[c, z], xe_sem.at[0], e, partner)
    for d in NEAR_FIRST:
        arrived(xe.at[c, at_z(NZ - d)], d_sem.at[d - 1])
        send(xe.at[c, at_z(NZ - d)], xe.at[c, at_z(NZ - d)], xe_sem.at[d], e, partner)
    sq = fsq[...]
    for d in NEAR_FIRST:
        arrived(fsqr.at[d - 1], fs_sem.at[d - 1])
        sq = sq + fsqr[d - 1]
    inverse = lax.rsqrt(sq / MODEL + EPSILON)
    inverse = jnp.concatenate([inverse[i : i + 1] for i in range(4)], axis=1)
    slot = iota((CAP, SEQS), 0) + e * CAP
    mine = (slots[0] == slot) | (slots[1] == slot)
    slot_scale = jnp.sum(jnp.where(mine, jnp.broadcast_to(inverse, (CAP, SEQS)), 0.0), axis=1, keepdims=True)
    own_row = iota((64, SEQS), 1) == iota((64, SEQS), 0) + z * 64
    row_scale = jnp.sum(jnp.where(own_row, jnp.broadcast_to(inverse, (64, SEQS)), 0.0), axis=1, keepdims=True)
    c_eg.wait()
    c_eu.wait()
    acc = jnp.zeros((CAP, 256), F32)
    for d in (0,) + NEAR_FIRST:
        zs = at_z(NZ - d)
        arrived(xe.at[1 - c, zs], xe_sem.at[d])
        rows = jnp.concatenate([xe[0, zs], xe[1, zs]], axis=0)
        both = jnp.concatenate([egb[zs], eub[zs]], axis=1)
        acc = acc + jnp.dot(rows, both, preferred_element_type=F32)
    acc = acc * slot_scale
    gate = acc[:, 0:128]
    hidden = (gate / (1.0 + jnp.exp(-gate)) * acc[:, 128:256]).astype(BF16)
    for copy in c_ed:
        copy.wait()
    for k, d in enumerate(FAR_FIRST + (0,)):
        zi = at_z(d)
        part = jnp.dot(hidden, edb[zi], preferred_element_type=F32)
        kept = jnp.where(c == 0, part[:HALF], part[HALF:]).astype(BF16)
        given = jnp.where(c == 0, part[HALF:], part[:HALF]).astype(BF16)
        for xi in range(NX):
            pown[zi, xi] = kept[:, xi * 128 : (xi + 1) * 128]
            pout[zi, xi] = given[:, xi * 128 : (xi + 1) * 128]
        send(pout.at[zi], precv.at[zi], p_sem.at[k], e, partner)

    gu = gub[z].astype(F32)
    for d in NEAR_FIRST:
        arrived(gurecv.at[d - 1], gu_sem.at[d - 1])
        gu = gu + gurecv[d - 1].astype(F32)
    gu = gu * row_scale
    gate = gu[:, 0:128]
    hd[x, z] = (gate / (1.0 + jnp.exp(-gate)) * gu[:, 128:256]).astype(BF16)
    for d in FAR_FIRST:
        send(hd.at[x, z], hd.at[x, z], hz_sem.at[d - 1], at_z(d) * NX + x, t)

    for k, d in enumerate(FAR_FIRST + (0,)):
        zi = at_z(d)
        arrived(precv.at[zi], p_sem.at[k])
        rsum[zi] = (pown[zi].astype(F32) + precv[zi].astype(F32)).astype(BF16)
        for dx in (2, 1, 3, 0):
            if d or dx:
                send(rsum.at[zi, at_x(dx)], rt.at[e], rt_sem.at[d * NX + dx], zi * NX + at_x(dx), t)
    rt[e] = rsum[z, x]

    for dx in (2, 1, 3):
        send(hd.at[x, z], hd.at[x, z], hx_sem.at[dx - 1], z * NX + at_x(dx), t)
    for d in NEAR_FIRST:
        zs = at_z(NZ - d)
        arrived(hd.at[x, zs], hz_sem.at[d - 1])
        for dx in (2, 1, 3):
            send(hd.at[x, zs], hd.at[x, zs], hx_sem.at[d * 3 + dx - 1], z * NX + at_x(dx), t)

    for d in range(NZ):
        for dx in range(NX):
            if d or dx:
                arrived(rt.at[at_z(NZ - d) * NX + at_x(NX - dx)], rt_sem.at[d * NX + dx])
    moe = lax.dot_general(ctm[...], rt[...].reshape(1024, 128), (((0,), (0,)), ((), ())), preferred_element_type=F32)
    for d in (0,) + NEAR_FIRST:
        for dx in (1, 3, 2):
            arrived(hd.at[at_x(NX - dx), at_z(NZ - d)], hx_sem.at[d * 3 + dx - 1])
    c_dd.wait()
    dense = jnp.zeros((SEQS, 128), F32)
    for xi in range(NX):
        dense = dense + jnp.dot(hd[xi].reshape(SEQS, 128), ddb[xi * 128 : (xi + 1) * 128], preferred_element_type=F32)
    fbuf[...] = (moe + mgain[...] * dense).astype(BF16).reshape(NT, 64, 128)

    for d in (4, 5, 3, 2, 6, 7, 1):
        send(fbuf.at[at_t(d)], frecv.at[d - 1], f_sem.at[d - 1], e, at_t(d))
    for d in (1, 2, 3):
        arrived(afin.at[at_x(NX - d)], af_sem.at[d - 1])
    out = jnp.concatenate([strm[xi, t].astype(F32) + afin[xi].astype(F32) for xi in range(NX)], axis=0)
    out = out + fbuf[t].astype(F32)
    for d in NEAR_FIRST:
        arrived(frecv.at[d - 1], f_sem.at[d - 1])
        out = out + frecv[d - 1].astype(F32)
    mgath[t] = out.astype(BF16)
    for d in (4, 5, 3, 2, 6, 7, 1):
        send(mgath.at[t], mgath.at[t], m_sem.at[d - 1], e, at_t(d))
    for d in NEAR_FIRST:
        arrived(mgath.at[at_t(NT - d)], m_sem.at[d - 1])
    mixed[...] = mgath[...].reshape(SEQS, 128)
    for copy in started:
        copy.wait_send()


def per_device(
    stream, norm_gain, w_query, w_key, w_value, break_offset, cache_keys, cache_values, lengths, w_output, head_gain,
    ffn_gain, route_experts, route_weights, expert_gate, expert_up, expert_down, dense_gate, dense_up, dense_down, mix_gain,
):
    any_spec = pl.BlockSpec(memory_space=pl.ANY)
    vm = pl.BlockSpec(memory_space=pltpu.VMEM)
    sm = pl.BlockSpec(memory_space=pltpu.SMEM)
    dma = pltpu.SemaphoreType.DMA

    def b(*shape):
        return pltpu.VMEM(shape, BF16)

    def f(*shape):
        return pltpu.VMEM(shape, F32)

    scratch = dict(
        strm=b(NX, NZ, ROWS, 128), wqkv=b(128, 512), kbuf=b(ROWS, LEN, 128), vbuf=b(ROWS, LEN, 128),
        ybuf=b(NX, 128, 512), yrecv=b(NX - 1, 128, 512), ssq=f(NX, 8, 128), ssqr=f(NX - 1, 8, 128),
        zbuf=b(NZ, ROWS, 512), zrecv=b(NZ - 1, ROWS, 512), zsq=f(8, 128), zsqr=f(NZ - 1, 8, 128),
        wog=b(NX, 256, 128), hall=b(NZ, ROWS, 256), obuf=b(NZ, ROWS, 512), orecv=b(NT - 1, ROWS, 512),
        abuf=b(NX, ROWS, 128), afin=b(NX, ROWS, 128), sres=b(NX, ROWS, 128), fgb=f(8, 128), fgall=f(NX, 8, 128),
        wgu=b(NX, 128, 256), ddb=b(512, 128), egb=b(NZ, 512, 128), eub=b(NZ, 512, 128), edb=b(NZ, 128, 512),
        pmat=b(256, SEQS), ctm=b(1024, SEQS), rbuf=b(ROWS, 512), rall=b(NT, NX, ROWS, 512), gbuf=b(SEQS, 512),
        fsq=f(8, 128), fsqr=f(NZ - 1, 8, 128), gub=b(NZ, 64, 256), gurecv=b(NZ - 1, 64, 256),
        dbuf=b(NZ, HALF, 512), xe=b(2, NZ, HALF, 512), hd=b(NX, NZ, 64, 128),
        pown=b(NZ, NX, HALF, 128), pout=b(NZ, NX, HALF, 128), precv=b(NZ, NX, HALF, 128), rsum=b(NZ, NX, HALF, 128),
        rt=b(32, HALF, 128), fbuf=b(NT, 64, 128), frecv=b(NT - 1, 64, 128), mgath=b(NT, 64, 128),
        lsem=dma((24,)), ssem=dma((208,)),
        yx_sem=dma((3,)), sx_sem=dma((3,)), wo_sem=dma((3,)), wg_sem=dma((3,)), wu_sem=dma((3,)), sr_sem=dma((3,)),
        fg_sem=dma((3,)), yz_sem=dma((7,)), sz_sem=dma((7,)), h_sem=dma((7,)), o_sem=dma((7,)), af_sem=dma((3,)),
        r_sem=dma((32,)), fs_sem=dma((7,)), gu_sem=dma((7,)), d_sem=dma((7,)), xe_sem=dma((8,)), hz_sem=dma((7,)),
        hx_sem=dma((24,)), p_sem=dma((8,)), rt_sem=dma((32,)), f_sem=dma((7,)), m_sem=dma((7,)),
    )
    return pl.pallas_call(
        step_kernel,
        name="step",
        out_shape=(
            jax.ShapeDtypeStruct((SEQS, 128), BF16),
            jax.ShapeDtypeStruct((ROWS, 128), BF16),
            jax.ShapeDtypeStruct((ROWS, 128), BF16),
        ),
        in_specs=[any_spec] * 13 + [vm] * 6 + [sm] * 2,
        out_specs=(vm, vm, vm),
        scratch_shapes=list(scratch.values()),
        compiler_params=pltpu.CompilerParams(collective_id=0, has_side_effects=True, vmem_limit_bytes=60 * 1024 * 1024),
    )(
        stream.reshape(NZ, NX, ROWS, 128), w_query, w_key, w_value,
        cache_keys.reshape(ROWS, LEN, 128), cache_values.reshape(ROWS, LEN, 128), w_output,
        expert_gate.reshape(NZ, 512, 128), expert_up.reshape(NZ, 512, 128), expert_down.reshape(128, MODEL),
        dense_gate, dense_up, dense_down,
        norm_gain.reshape(1, 128), head_gain.reshape(2, 128), ffn_gain.reshape(1, 128), mix_gain.reshape(1, 128),
        route_experts.T, route_weights.T, break_offset, lengths,
    )


def solution(mesh):
    in_specs = (
        P(None, "ep"),
        P("ep"),
        P("ep", "tp"),
        P("ep", "tp"),
        P("ep", "tp"),
        P("tp"),
        P("ep", None, "tp", None),
        P("ep", None, "tp", None),
        P("ep"),
        P("tp", "ep"),
        P("tp"),
        P("ep"),
        P(),
        P(),
        P("ep", None, "tp"),
        P("ep", None, "tp"),
        P("ep", "tp", None),
        P("ep", "tp"),
        P("ep", "tp"),
        P("tp", "ep"),
        P("ep"),
    )
    out_specs = (P(None, "ep"), P("ep", "tp"), P("ep", "tp"))
    return jax.shard_map(
        per_device, mesh=mesh, in_specs=in_specs, out_specs=out_specs, check_vma=False
    )
```

time: 238 us -> 93.9 us (0.39)
  Pallas kernels: 44.6 us -> 88.9 us
  starting transfers between devices: 40.6 us -> 0 us
  waiting for transfers between devices: 40.6 us -> 0 us
  other arithmetic: 39.1 us -> 0 us
  blocking collectives: 33.3 us -> 0 us
  local copies, waits for them, and re-layouts: 31.8 us -> 4.11 us
  matrix products: 5.72 us -> 0 us
    pallas_call x1, Pallas kernels: 44.6 us -> 88.9 us  [per_device(): pl.pallas_call(step_kernel, name='step', out_shape=(jax.ShapeDtypeStruct(...]
    all_to_all x7 -> x0, waiting for transfers between devices: 40.6 us -> none  [the longest x4 25.3 us: sent_to_all(): lax.all_to_all(jnp.broadcast_to(x[None], (size, *x.shape)), axis, 0, 0, t...]
    all_to_all x7 -> x0, starting transfers between devices: 40.6 us -> none  [the longest x4 23.3 us: sent_to_all(): lax.all_to_all(jnp.broadcast_to(x[None], (size, *x.shape)), axis, 0, 0, t...]
    unnamed x1 -> x0, other arithmetic: 23.4 us -> none
    all_to_all x1 -> x0, blocking collectives: 18 us -> none  [per_device(): lax.all_to_all(own_slots, 'ep', split_axis=0, concat_axis=2, tiled=True)]
    all_gather x1 -> x0, blocking collectives: 15.3 us -> none  [per_device(): gathered = lax.all_gather(arrived, 'tp', axis=1, tiled=True)]
    gather x2 -> x0, local copies, waits for them, and re-layouts: 9.39 us -> none  [the longest x1 6.18 us: per_device(): outgoing = padded[filled].reshape(experts, capacity, block_width)]
    another operation x3 -> x0, other arithmetic: 9.15 us -> none
  transfers between devices with their start and end apart: 7 -> 0, of which waited for: 5 -> 0; matrix products, arithmetic and copies ran while one was open for 26% -> 0% of each run, Pallas kernels for 0% -> 0%
where the time goes in v2:
time: 93.9 us; the launch traced here: 93.6 us
  Pallas kernels  88.9 us (95%)
  local copies, waits for them, and re-layouts  4.11 us (4%)
    pallas_call x1, Pallas kernels, per_device(): pl.pallas_call(step_kernel, name='step', out_shape=(jax.ShapeDtypeStruct(...  88.9 us
    unnamed x3, local copies, waits for them, and re-layouts  4.11 us

profile of v2, /device:TPU:1, one launch (start us, length us, event | category | flops | bytes accessed | tf_op | source)
XLA Modules:
  0.0 93.6 jit_solution(17645611858294956745)
XLA Ops:
  0.6 88.9 %step.1 = (bf16[512,128]{1,0:T(8,128)(2,1)}, bf16[16,128]{1,0:T(8,128)(2,1)}, bf16[16,128]{1,0:T(8,128)(2,1)}) custom-call(bf16[8,4,16,128]{3,2,1,0:T(8,128)(2,1)} %bitcast.17, bf16[128,256]{1,0:T(8,128)(2,1)} %wq.1, bf16[128,128]{1,0:T(8,128)(2,1)} %wk.1, bf16[128,128]{1,0:T(8,128)(2,1)} %wv.1, bf16[16,1024,128]{2,1,0:T(8,128)(2,1)} %bitcast.12, ...), custom_call_target="tpu_custom_call" | custom-call | tf_op jit(solution)/shard_map/step/pallas_call | solution.py:404
  89.5 1.6 %copy.27 = bf16[512,128]{1,0:T(8,128)(2,1)} copy(bf16[512,128]{1,0:T(8,128)(2,1)} %get-tuple-element.6) | data formatting | bytes 262144
  91.1 1.3 %copy.28 = bf16[16,128]{1,0:T(8,128)(2,1)} copy(bf16[16,128]{1,0:T(8,128)(2,1)} %get-tuple-element.7) | data formatting | bytes 8192
  92.4 1.3 %copy.29 = bf16[16,128]{1,0:T(8,128)(2,1)} copy(bf16[16,128]{1,0:T(8,128)(2,1)} %get-tuple-element.8) | data formatting | bytes 8192

commit v3 on v2

--- a/solution.py
+++ b/solution.py
@@ -22,14 +22,15 @@
 
 def step_kernel(
     stream, wq, wk, wv, ck, cv, wo, eg, eu, ed, dg, du, dd,
+    ngain_hbm, hgain_hbm, fgain_hbm, mgain_hbm, route_hbm, rweights_hbm, boff_hbm, lens_hbm,
+    mixed, key_rows, value_rows,
     ngain, hgain, fgain, mgain, route, rweights, boff, lens,
-    mixed, key_rows, value_rows,
-    strm, wqkv, kbuf, vbuf, ybuf, yrecv, ssq, ssqr, zbuf, zrecv, zsq, zsqr,
-    wog, hall, obuf, orecv, abuf, afin, sres, fgb, fgall, wgu, ddb, egb, eub, edb,
+    strm, wqkv, kbuf, vbuf, xgain, yq, yqr, yk, ykr, ssq, ssqr, zq, zqr, zk, zkr, zsq, zsqr,
+    wog, hall, obuf, orecv, sres, fgb, fgall, wgu, ddb, egb, eub, edb,
     pmat, ctm, rbuf, rall, gbuf, fsq, fsqr, gub, gurecv, dbuf, xe, hd,
-    pown, pout, precv, rsum, rt, fbuf, frecv, mgath,
-    lsem, ssem,
-    yx_sem, sx_sem, wo_sem, wg_sem, wu_sem, sr_sem, fg_sem, yz_sem, sz_sem, h_sem, o_sem, af_sem, r_sem,
+    pown, pout, precv, rsum, rt, fbuf, fpair, fhalf, frecv, mgath,
+    lsem, ssem, ring_sem,
+    yq_sem, yk_sem, sx_sem, wo_sem, wg_sem, wu_sem, sr_sem, fg_sem, zq_sem, zk_sem, sz_sem, h_sem, o_sem, r_sem, rf_sem,
     fs_sem, gu_sem, d_sem, xe_sem, hz_sem, hx_sem, p_sem, rt_sem, f_sem, m_sem,
 ):
     e = lax.axis_index("ep")
@@ -72,18 +73,22 @@
     def columns(ref, block):
         return ref.at[:, pl.ds(pl.multiple_of(block * 128, 128), 128)]
 
-    c_w = [load(wq, wqkv.at[:, 0:256]), load(wk, wqkv.at[:, 256:384]), load(wv, wqkv.at[:, 384:512])]
+    def signal(sem, dev_e, dev_t):
+        pl.semaphore_signal(sem, inc=1, device_id=(dev_e, dev_t), device_id_type=MESH)
+
+    barrier = pltpu.get_barrier_semaphore()
+    for d in (1, NZ - 1):
+        signal(barrier, at_z(d) * NX + x, t)
+    for d in range(1, NX):
+        signal(barrier, z * NX + at_x(d), t)
+    for d in range(1, NT):
+        signal(barrier, e, at_t(d))
+
     c_s = [load(stream.at[:, xi], strm.at[xi]) for xi in range(NX)]
-
-    barrier = pltpu.get_barrier_semaphore()
-    peers = 0
-    for dt in range(NT):
-        for dz in range(NZ):
-            for dx in range(NX):
-                if (dt == 0 and (dz or dx)) or (dt and dz == 0):
-                    pl.semaphore_signal(barrier, inc=1, device_id=(at_z(dz) * NX + at_x(dx), at_t(dt)), device_id_type=MESH)
-                    peers += 1
-
+    c_w = [load(ngain_hbm, ngain), load(wq, wqkv.at[:, 0:256]), load(wk, wqkv.at[:, 256:384]), load(wv, wqkv.at[:, 384:512])]
+    c_route = [load(route_hbm, route), load(rweights_hbm, rweights)]
+    c_small = [load(hgain_hbm, hgain), load(mgain_hbm, mgain), load(boff_hbm, boff), load(lens_hbm, lens)]
+    c_fg = load(fgain_hbm, fgain)
     c_wo = load(wo, wog.at[x])
     c_k = load(ck, kbuf)
     c_v = load(cv, vbuf)
@@ -94,34 +99,72 @@
     c_eu = load(eu, eub)
     c_ed = [load(ed.at[:, zi * 512 : (zi + 1) * 512], edb.at[zi]) for zi in range(NZ)]
 
-    for copy in c_w + c_s:
+    for copy in c_s + c_w:
         copy.wait()
     gain = ngain[...]
     w = wqkv[...]
     for xi in range(NX):
         rows = strm[xi].reshape(NZ * ROWS, HD).astype(F32)
-        ybuf[xi] = jnp.dot((rows * gain).astype(BF16), w, preferred_element_type=F32).astype(BF16)
+        scaled = (rows * gain).astype(BF16)
+        xgain[xi] = scaled
+        yq[xi] = jnp.dot(scaled, w[:, 0:256], preferred_element_type=F32).astype(BF16).reshape(NZ, ROWS, 256)
         sums = jnp.sum((rows * rows).T, axis=0, keepdims=True)
         ssq[xi] = jnp.broadcast_to(sums, (8, HD))
+    c_fg.wait()
     fgb[...] = jnp.broadcast_to(fgain[...], (8, HD))
 
-    pl.semaphore_wait(barrier, peers)
+    pl.semaphore_wait(barrier, 2 + NX - 1 + NT - 1)
 
     for d in (2, 1, 3):
-        to = z * NX + at_x(d)
-        send(ybuf.at[at_x(d)], yrecv.at[d - 1], yx_sem.at[d - 1], to, t)
-        send(ssq.at[at_x(d)], ssqr.at[d - 1], sx_sem.at[d - 1], to, t)
+        send(ssq.at[at_x(d)], ssqr.at[d - 1], sx_sem.at[d - 1], z * NX + at_x(d), t)
+    for k in FAR_FIRST + (0,):
+        for d in (2, 1, 3):
+            send(yq.at[at_x(d), at_z(k)], yqr.at[d - 1, k], yq_sem.at[k * 3 + d - 1], z * NX + at_x(d), t)
+    signal(ring_sem.at[0], at_z(1) * NX + x, t)
+    signal(ring_sem.at[1], at_z(7) * NX + x, t)
     c_wo.wait()
     for d in (2, 1, 3):
         to = z * NX + at_x(d)
         send(wog.at[x], wog.at[x], wo_sem.at[d - 1], to, t)
         send(strm.at[at_x(d), t], sres.at[x], sr_sem.at[d - 1], to, t)
         send(fgb, fgall.at[x], fg_sem.at[d - 1], to, t)
+    sres[x] = strm[x, t]
+    fgall[x] = fgb[...]
+    pl.semaphore_wait(ring_sem.at[0], 1)
+    pl.semaphore_wait(ring_sem.at[1], 1)
+    signal(ring_sem.at[2], at_z(2) * NX + x, t)
+    signal(ring_sem.at[3], at_z(6) * NX + x, t)
+    for xi in range(NX):
+        yk[xi] = jnp.dot(xgain[xi], w[:, 256:512], preferred_element_type=F32).astype(BF16).reshape(NZ, ROWS, 256)
+    for d in (2, 1, 3):
+        send(yk.at[at_x(d)], ykr.at[d - 1], yk_sem.at[d - 1], z * NX + at_x(d), t)
+    for d in (2, 1, 3):
+        to = z * NX + at_x(d)
         send(columns(dg, at_x(d)), wgu.at[x, :, 0:128], wg_sem.at[d - 1], to, t)
         send(columns(du, at_x(d)), wgu.at[x, :, 128:256], wu_sem.at[d - 1], to, t)
-    sres[x] = strm[x, t]
-    fgall[x] = fgb[...]
-
+    pl.semaphore_wait(ring_sem.at[2], 1)
+    pl.semaphore_wait(ring_sem.at[3], 1)
+
+    sq = ssq[x]
+    for d in (1, 3, 2):
+        arrived(ssqr.at[d - 1], sx_sem.at[d - 1])
+        sq = sq + ssqr[d - 1]
+    zsq[...] = sq
+    for d in FAR_FIRST:
+        send(zsq, zsqr.at[d - 1], sz_sem.at[d - 1], at_z(d) * NX + x, t)
+    for k in FAR_FIRST + (0,):
+        total = yq[x, at_z(k)].astype(F32)
+        for d in (1, 3, 2):
+            arrived(yqr.at[d - 1, k], yq_sem.at[k * 3 + d - 1])
+            total = total + yqr[d - 1, k].astype(F32)
+        if k:
+            zq[k - 1] = total.astype(BF16)
+            send(zq.at[k - 1], zqr.at[k - 1], zq_sem.at[k - 1], at_z(k) * NX + x, t)
+        else:
+            queries = total
+
+    for copy in c_route:
+        copy.wait()
     names = [route[0:1], route[1:2]]
     expert = iota((32, SEQS), 0)
     chosen = (jnp.where(names[0] == expert, 1.0, 0.0) + jnp.where(names[1] == expert, 1.0, 0.0)).astype(BF16)
@@ -143,35 +186,19 @@
             slots[0] == slot, shares[0], jnp.where(slots[1] == slot, shares[1], 0.0)
         ).astype(BF16)
 
-    total = ybuf[x].astype(F32)
-    sq = ssq[x]
-    for d in (1, 3, 2):
-        arrived(yrecv.at[d - 1], yx_sem.at[d - 1])
-        arrived(ssqr.at[d - 1], sx_sem.at[d - 1])
-        total = total + yrecv[d - 1].astype(F32)
-        sq = sq + ssqr[d - 1]
-    zbuf[...] = total.astype(BF16).reshape(NZ, ROWS, 512)
-    zsq[...] = sq
-
-    for d in FAR_FIRST:
-        to = at_z(d) * NX + x
-        send(zbuf.at[at_z(d)], zrecv.at[d - 1], yz_sem.at[d - 1], to, t)
-        send(zsq, zsqr.at[d - 1], sz_sem.at[d - 1], to, t)
-    qkv = zbuf[z].astype(F32)
     sq = zsq[...]
     for d in NEAR_FIRST:
-        arrived(zrecv.at[d - 1], yz_sem.at[d - 1])
+        arrived(zqr.at[d - 1], zq_sem.at[d - 1])
         arrived(zsqr.at[d - 1], sz_sem.at[d - 1])
-        qkv = qkv + zrecv[d - 1].astype(F32)
+        queries = queries + zqr[d - 1].astype(F32)
         sq = sq + zsqr[d - 1]
     lane = iota((ROWS, HD), 1)
     pick = lane == z * ROWS + iota((ROWS, HD), 0)
     mean = jnp.sum(jnp.where(pick, jnp.broadcast_to(sq[0:1], (ROWS, HD)), 0.0), axis=1, keepdims=True) / MODEL
-    qkv = qkv * lax.rsqrt(mean + EPSILON)
-    key_rows[...] = qkv[:, 256:384].astype(BF16)
-    value_rows[...] = qkv[:, 384:512].astype(BF16)
-
-    q = jnp.concatenate([qkv[:, 0:128], qkv[:, 128:256]], axis=0).astype(BF16).astype(F32)
+    token_scale = lax.rsqrt(mean + EPSILON)
+    queries = queries * token_scale
+
+    q = jnp.concatenate([queries[:, 0:128], queries[:, 128:256]], axis=0).astype(BF16).astype(F32)
     seq = lax.rem(iota((2 * ROWS, 1), 0), ROWS)
     c_k.wait()
     scores = jnp.zeros((2 * ROWS, LEN), F32)
@@ -180,6 +207,8 @@
         own = jnp.concatenate([jnp.where(seq == 2 * p, q, 0.0), jnp.where(seq == 2 * p + 1, q, 0.0)], axis=1)
         scores = scores + lax.dot_general(own.astype(BF16), keys, (((1,), (1,)), ((), ())), preferred_element_type=F32)
     first = iota((2 * ROWS, 1), 0) < ROWS
+    for copy in c_small:
+        copy.wait()
     length = jnp.zeros((2 * ROWS, 1), jnp.int32)
     for s in range(ROWS):
         length = jnp.where(seq == s, lens[s], length)
@@ -209,6 +238,13 @@
 
     for d in FAR_FIRST:
         send(hall.at[z], hall.at[z], h_sem.at[d - 1], at_z(d) * NX + x, t)
+    kv = yk[x].astype(F32)
+    for d in (1, 3, 2):
+        arrived(ykr.at[d - 1], yk_sem.at[d - 1])
+        kv = kv + ykr[d - 1].astype(F32)
+    zk[...] = kv.astype(BF16)
+    for d in FAR_FIRST:
+        send(zk.at[at_z(d)], zkr.at[d - 1], zk_sem.at[d - 1], at_z(d) * NX + x, t)
     for d in (1, 2, 3):
         arrived(wog.at[at_x(NX - d)], wo_sem.at[d - 1])
         arrived(sres.at[at_x(NX - d)], sr_sem.at[d - 1])
@@ -231,21 +267,33 @@
         attn = attn + orecv[d - 1].astype(F32)
     attn = attn.astype(BF16)
     rbuf[...] = (attn.astype(F32) + jnp.concatenate([sres[xi].astype(F32) for xi in range(NX)], axis=1)).astype(BF16)
-    for xi in range(NX):
-        abuf[xi] = attn[:, xi * 128 : (xi + 1) * 128]
-
-    for dt in (4, 5, 3, 2, 6, 7, 1, 0):
+
+    def at_y(d):
+        return lax.rem(t + 2 * d, NT)
+
+    for dy in (2, 1, 3, 0):
         for dx in (2, 1, 3, 0):
-            if dt or dx:
-                send(rbuf, rall.at[t, x], r_sem.at[dt * NX + dx], z * NX + at_x(dx), at_t(dt))
-    for d in (2, 1, 3):
-        send(abuf.at[at_x(d)], afin.at[x], af_sem.at[d - 1], z * NX + at_x(d), t)
+            if dy or dx:
+                send(rbuf, rall.at[t, x], r_sem.at[dy * NX + dx], z * NX + at_x(dx), at_y(dy))
+    send(rbuf, rall.at[t, x], rf_sem.at[0], e, partner)
     rall[t, x] = rbuf[...]
-    afin[x] = abuf[x]
-    for dt in range(NT):
+    kv = zk[z].astype(F32)
+    for d in NEAR_FIRST:
+        arrived(zkr.at[d - 1], zk_sem.at[d - 1])
+        kv = kv + zkr[d - 1].astype(F32)
+    kv = kv * token_scale
+    key_rows[...] = kv[:, 0:128].astype(BF16)
+    value_rows[...] = kv[:, 128:256].astype(BF16)
+    for dy in (0, 1, 3, 2):
+        for dx in (0, 1, 3, 2):
+            if dy or dx:
+                block = rall.at[at_y(4 - dy), at_x(NX - dx)]
+                arrived(block, r_sem.at[dy * NX + dx])
+                send(block, block, rf_sem.at[dy * NX + dx], e, partner)
+    other = lax.div(t, 2) * 2 + 1 - c
+    for dy in range(4):
         for dx in range(NX):
-            if dt or dx:
-                arrived(rall.at[at_t(NT - dt), at_x(NX - dx)], r_sem.at[dt * NX + dx])
+            arrived(rall.at[lax.rem(other + 2 * (4 - dy), NT), at_x(NX - dx)], rf_sem.at[dy * NX + dx])
     gains = jnp.concatenate([fgall[xi][0:1] for xi in range(NX)], axis=1)
     square_rows = []
     for i in range(4):
@@ -347,25 +395,32 @@
     dense = jnp.zeros((SEQS, 128), F32)
     for xi in range(NX):
         dense = dense + jnp.dot(hd[xi].reshape(SEQS, 128), ddb[xi * 128 : (xi + 1) * 128], preferred_element_type=F32)
-    fbuf[...] = (moe + mgain[...] * dense).astype(BF16).reshape(NT, 64, 128)
-
-    for d in (4, 5, 3, 2, 6, 7, 1):
-        send(fbuf.at[at_t(d)], frecv.at[d - 1], f_sem.at[d - 1], e, at_t(d))
-    for d in (1, 2, 3):
-        arrived(afin.at[at_x(NX - d)], af_sem.at[d - 1])
-    out = jnp.concatenate([strm[xi, t].astype(F32) + afin[xi].astype(F32) for xi in range(NX)], axis=0)
-    out = out + fbuf[t].astype(F32)
-    for d in NEAR_FIRST:
-        arrived(frecv.at[d - 1], f_sem.at[d - 1])
+    fbuf[...] = (moe + mgain[...] * dense).astype(BF16).reshape(2, 256, 128)
+
+    send(fbuf.at[1 - c], fpair, f_sem.at[0], e, partner)
+    out = fbuf[c].astype(F32)
+    arrived(fpair, f_sem.at[0])
+    out = out + fpair[...].astype(F32)
+    fhalf[...] = out.astype(BF16)
+    for d in (2, 1, 3):
+        send(fhalf, frecv.at[d - 1], f_sem.at[d], e, at_y(d))
+    mine = pl.ds(pl.multiple_of(x * 128, 128), 128)
+    out = out + rall[pl.ds(c * 4, 4), :, :, mine].reshape(256, 128).astype(F32)
+    for d in (1, 3, 2):
+        arrived(frecv.at[d - 1], f_sem.at[d])
         out = out + frecv[d - 1].astype(F32)
-    mgath[t] = out.astype(BF16)
-    for d in (4, 5, 3, 2, 6, 7, 1):
-        send(mgath.at[t], mgath.at[t], m_sem.at[d - 1], e, at_t(d))
-    for d in NEAR_FIRST:
-        arrived(mgath.at[at_t(NT - d)], m_sem.at[d - 1])
+    mgath[c] = out.astype(BF16)
+    send(mgath.at[c], mgath.at[c], m_sem.at[0], e, partner)
+    arrived(mgath.at[1 - c], m_sem.at[0])
     mixed[...] = mgath[...].reshape(SEQS, 128)
     for copy in started:
         copy.wait_send()
+
+
+def finish_kernel(a, b, c, a_out, b_out, c_out):
+    a_out[...] = a[...]
+    b_out[...] = b[...]
+    c_out[...] = c[...]
 
 
 def per_device(
@@ -374,7 +429,6 @@
 ):
     any_spec = pl.BlockSpec(memory_space=pl.ANY)
     vm = pl.BlockSpec(memory_space=pltpu.VMEM)
-    sm = pl.BlockSpec(memory_space=pltpu.SMEM)
     dma = pltpu.SemaphoreType.DMA
 
     def b(*shape):
@@ -384,24 +438,29 @@
         return pltpu.VMEM(shape, F32)
 
     scratch = dict(
+        ngain=f(1, 128), hgain=f(2, 128), fgain=f(1, 128), mgain=f(1, 128),
+        route=pltpu.VMEM((2, SEQS), jnp.int32), rweights=f(2, SEQS), boff=pltpu.SMEM((2,), F32), lens=pltpu.SMEM((ROWS,), jnp.int32),
         strm=b(NX, NZ, ROWS, 128), wqkv=b(128, 512), kbuf=b(ROWS, LEN, 128), vbuf=b(ROWS, LEN, 128),
-        ybuf=b(NX, 128, 512), yrecv=b(NX - 1, 128, 512), ssq=f(NX, 8, 128), ssqr=f(NX - 1, 8, 128),
-        zbuf=b(NZ, ROWS, 512), zrecv=b(NZ - 1, ROWS, 512), zsq=f(8, 128), zsqr=f(NZ - 1, 8, 128),
+        xgain=b(NX, 128, 128), yq=b(NX, NZ, ROWS, 256), yqr=b(NX - 1, NZ, ROWS, 256),
+        yk=b(NX, NZ, ROWS, 256), ykr=b(NX - 1, NZ, ROWS, 256), ssq=f(NX, 8, 128), ssqr=f(NX - 1, 8, 128),
+        zq=b(NZ - 1, ROWS, 256), zqr=b(NZ - 1, ROWS, 256), zk=b(NZ, ROWS, 256), zkr=b(NZ - 1, ROWS, 256),
+        zsq=f(8, 128), zsqr=f(NZ - 1, 8, 128),
         wog=b(NX, 256, 128), hall=b(NZ, ROWS, 256), obuf=b(NZ, ROWS, 512), orecv=b(NT - 1, ROWS, 512),
-        abuf=b(NX, ROWS, 128), afin=b(NX, ROWS, 128), sres=b(NX, ROWS, 128), fgb=f(8, 128), fgall=f(NX, 8, 128),
+        sres=b(NX, ROWS, 128), fgb=f(8, 128), fgall=f(NX, 8, 128),
         wgu=b(NX, 128, 256), ddb=b(512, 128), egb=b(NZ, 512, 128), eub=b(NZ, 512, 128), edb=b(NZ, 128, 512),
         pmat=b(256, SEQS), ctm=b(1024, SEQS), rbuf=b(ROWS, 512), rall=b(NT, NX, ROWS, 512), gbuf=b(SEQS, 512),
         fsq=f(8, 128), fsqr=f(NZ - 1, 8, 128), gub=b(NZ, 64, 256), gurecv=b(NZ - 1, 64, 256),
         dbuf=b(NZ, HALF, 512), xe=b(2, NZ, HALF, 512), hd=b(NX, NZ, 64, 128),
         pown=b(NZ, NX, HALF, 128), pout=b(NZ, NX, HALF, 128), precv=b(NZ, NX, HALF, 128), rsum=b(NZ, NX, HALF, 128),
-        rt=b(32, HALF, 128), fbuf=b(NT, 64, 128), frecv=b(NT - 1, 64, 128), mgath=b(NT, 64, 128),
-        lsem=dma((24,)), ssem=dma((208,)),
-        yx_sem=dma((3,)), sx_sem=dma((3,)), wo_sem=dma((3,)), wg_sem=dma((3,)), wu_sem=dma((3,)), sr_sem=dma((3,)),
-        fg_sem=dma((3,)), yz_sem=dma((7,)), sz_sem=dma((7,)), h_sem=dma((7,)), o_sem=dma((7,)), af_sem=dma((3,)),
-        r_sem=dma((32,)), fs_sem=dma((7,)), gu_sem=dma((7,)), d_sem=dma((7,)), xe_sem=dma((8,)), hz_sem=dma((7,)),
-        hx_sem=dma((24,)), p_sem=dma((8,)), rt_sem=dma((32,)), f_sem=dma((7,)), m_sem=dma((7,)),
+        rt=b(32, HALF, 128), fbuf=b(2, 256, 128), fpair=b(256, 128), fhalf=b(256, 128), frecv=b(3, 256, 128), mgath=b(2, 256, 128),
+        lsem=dma((32,)), ssem=dma((224,)), ring_sem=pltpu.SemaphoreType.REGULAR((4,)),
+        yq_sem=dma((24,)), yk_sem=dma((3,)), sx_sem=dma((3,)), wo_sem=dma((3,)), wg_sem=dma((3,)), wu_sem=dma((3,)),
+        sr_sem=dma((3,)), fg_sem=dma((3,)), zq_sem=dma((7,)), zk_sem=dma((7,)), sz_sem=dma((7,)), h_sem=dma((7,)), o_sem=dma((7,)),
+        r_sem=dma((16,)), rf_sem=dma((16,)),
+        fs_sem=dma((7,)), gu_sem=dma((7,)), d_sem=dma((7,)), xe_sem=dma((8,)), hz_sem=dma((7,)),
+        hx_sem=dma((24,)), p_sem=dma((8,)), rt_sem=dma((32,)), f_sem=dma((4,)), m_sem=dma((1,)),
     )
-    return pl.pallas_call(
+    results = pl.pallas_call(
         step_kernel,
         name="step",
         out_shape=(
@@ -409,7 +468,7 @@
             jax.ShapeDtypeStruct((ROWS, 128), BF16),
             jax.ShapeDtypeStruct((ROWS, 128), BF16),
         ),
-        in_specs=[any_spec] * 13 + [vm] * 6 + [sm] * 2,
+        in_specs=[any_spec] * 21,
         out_specs=(vm, vm, vm),
         scratch_shapes=list(scratch.values()),
         compiler_params=pltpu.CompilerParams(collective_id=0, has_side_effects=True, vmem_limit_bytes=60 * 1024 * 1024),
@@ -421,6 +480,13 @@
         norm_gain.reshape(1, 128), head_gain.reshape(2, 128), ffn_gain.reshape(1, 128), mix_gain.reshape(1, 128),
         route_experts.T, route_weights.T, break_offset, lengths,
     )
+    return pl.pallas_call(
+        finish_kernel,
+        name="finish",
+        out_shape=tuple(jax.ShapeDtypeStruct(r.shape, r.dtype) for r in results),
+        in_specs=[vm] * 3,
+        out_specs=(vm,) * 3,
+    )(*results)
 
 
 def solution(mesh):

time: 93.9 us -> 81.4 us (0.87)
  Pallas kernels: 88.9 us -> 80.6 us
  local copies, waits for them, and re-layouts: 4.11 us -> 0 us
    pallas_call x1, Pallas kernels: 88.9 us -> 79 us  [per_device(): pl.pallas_call(step_kernel, name='step', out_shape=(jax.ShapeDtypeStruct(...]
    unnamed x3 -> x0, local copies, waits for them, and re-layouts: 4.11 us -> none
    pallas_call x0 -> x1, Pallas kernels: none -> 1.58 us  [per_device(): pl.pallas_call(finish_kernel, name='finish', out_shape=tuple((jax.ShapeDt...]
where the time goes in v3:
time: 81.4 us; the launch traced here: 81.3 us
  Pallas kernels  80.6 us (99%)
    pallas_call x1, Pallas kernels, per_device(): pl.pallas_call(step_kernel, name='step', out_shape=(jax.ShapeDtypeStruct(...  79 us

profile of v3, /device:TPU:1, one launch (start us, length us, event | category | flops | bytes accessed | tf_op | source)
XLA Modules:
  0.0 81.3 jit_solution(10223905597936800614)
XLA Ops:
  0.6 79.0 %step.1 = (bf16[512,128]{1,0:T(8,128)(2,1)}, bf16[16,128]{1,0:T(8,128)(2,1)}, bf16[16,128]{1,0:T(8,128)(2,1)}) custom-call(bf16[8,4,16,128]{3,2,1,0:T(8,128)(2,1)} %bitcast.17, bf16[128,256]{1,0:T(8,128)(2,1)} %wq.1, bf16[128,128]{1,0:T(8,128)(2,1)} %wk.1, bf16[128,128]{1,0:T(8,128)(2,1)} %wv.1, bf16[16,1024,128]{2,1,0:T(8,128)(2,1)} %bitcast.12, ...), custom_call_target="tpu_custom_call" | custom-call | tf_op jit(solution)/shard_map/step/pallas_call | solution.py:463
  79.7 1.6 %finish.1 = (bf16[512,128]{1,0:T(8,128)(2,1)}, bf16[16,128]{1,0:T(8,128)(2,1)}, bf16[16,128]{1,0:T(8,128)(2,1)}) custom-call(bf16[512,128]{1,0:T(8,128)(2,1)} %get-tuple-element.6.a, bf16[16,128]{1,0:T(8,128)(2,1)} %get-tuple-element.7.b, bf16[16,128]{1,0:T(8,128)(2,1)} %get-tuple-element.8.c), custom_call_target="tpu_custom_call" | custom-call | tf_op jit(solution)/shard_map/finish/pallas_call | solution.py:483

commit v4 on v3

--- a/solution.py
+++ b/solution.py
@@ -28,10 +28,10 @@
     strm, wqkv, kbuf, vbuf, xgain, yq, yqr, yk, ykr, ssq, ssqr, zq, zqr, zk, zkr, zsq, zsqr,
     wog, hall, obuf, orecv, sres, fgb, fgall, wgu, ddb, egb, eub, edb,
     pmat, ctm, rbuf, rall, gbuf, fsq, fsqr, gub, gurecv, dbuf, xe, hd,
-    pown, pout, precv, rsum, rt, fbuf, fpair, fhalf, frecv, mgath,
+    pown, pout, precv, rsum, ysum, back, rt, fbuf, fpair, fhalf, frecv, mgath,
     lsem, ssem, ring_sem,
     yq_sem, yk_sem, sx_sem, wo_sem, wg_sem, wu_sem, sr_sem, fg_sem, zq_sem, zk_sem, sz_sem, h_sem, o_sem, r_sem, rf_sem,
-    fs_sem, gu_sem, d_sem, xe_sem, hz_sem, hx_sem, p_sem, rt_sem, f_sem, m_sem,
+    fs_sem, gu_sem, d_sem, xy_sem, xe_sem, hz_sem, hx_sem, p_sem, ys_sem, rt_sem, f_sem, m_sem,
 ):
     e = lax.axis_index("ep")
     t = lax.axis_index("tp")
@@ -175,13 +175,13 @@
     ]
     weight_sum = rweights[0:1] + rweights[1:2]
     shares = [rweights[0:1] / weight_sum, rweights[1:2] / weight_sum]
+    y = lax.div(t, 2)
+    row = iota((64, SEQS), 0)
+    slot = lax.shift_right_logical(row, 3) * (NX * CAP) + (x * CAP + c * HALF + y * 8) + (row & 7)
+    pmat[...] = jnp.where((slots[0] == slot) | (slots[1] == slot), 1.0, 0.0).astype(BF16)
     for i in range(2):
         row = iota((128, SEQS), 0) + i * 128
-        slot = lax.shift_right_logical(row, 5) * (NX * CAP) + (x * CAP + c * HALF) + (row & 31)
-        pmat[i * 128 : (i + 1) * 128] = jnp.where((slots[0] == slot) | (slots[1] == slot), 1.0, 0.0).astype(BF16)
-    for i in range(8):
-        row = iota((128, SEQS), 0) + i * 128
-        slot = lax.shift_right_logical(row, 5) * CAP + c * HALF + (row & 31)
+        slot = lax.shift_right_logical(row, 3) * CAP + c * HALF + y * 8 + (row & 7)
         ctm[i * 128 : (i + 1) * 128] = jnp.where(
             slots[0] == slot, shares[0], jnp.where(slots[1] == slot, shares[1], 0.0)
         ).astype(BF16)
@@ -304,12 +304,12 @@
         square_rows.append(jnp.sum(squares.T, axis=0, keepdims=True))
     fsq[...] = jnp.concatenate(square_rows + [jnp.zeros((4, 128), F32)], axis=0)
     dispatched = jnp.dot(pmat[...], gbuf[...], preferred_element_type=F32)
-    dbuf[...] = dispatched.astype(BF16).reshape(NZ, HALF, 512)
+    dbuf[...] = dispatched.reshape(NZ, 8, 512).astype(BF16)
     for d in FAR_FIRST:
         to = at_z(d) * NX + x
-        send(dbuf.at[at_z(d)], xe.at[c, z], d_sem.at[d - 1], to, t)
+        send(dbuf.at[at_z(d)], xe.at[t, z], d_sem.at[d - 1], to, t)
         send(fsq, fsqr.at[d - 1], fs_sem.at[d - 1], to, t)
-    xe[c, z] = dbuf[z]
+    xe[t, z] = dbuf[z]
     wide = wgu[...].reshape(512, 256)
     for i in range(4):
         part = jnp.dot(gbuf[i * 128 : (i + 1) * 128], wide, preferred_element_type=F32)
@@ -317,10 +317,16 @@
     for d in FAR_FIRST:
         send(gub.at[at_z(d)], gurecv.at[d - 1], gu_sem.at[d - 1], at_z(d) * NX + x, t)
 
-    send(xe.at[c, z], xe.at[c, z], xe_sem.at[0], e, partner)
-    for d in NEAR_FIRST:
-        arrived(xe.at[c, at_z(NZ - d)], d_sem.at[d - 1])
-        send(xe.at[c, at_z(NZ - d)], xe.at[c, at_z(NZ - d)], xe_sem.at[d], e, partner)
+    def spread(d):
+        block = xe.at[t, at_z(NZ - d)]
+        if d:
+            arrived(block, d_sem.at[d - 1])
+        for dy in (2, 1, 3):
+            send(block, block, xy_sem.at[d * 3 + dy - 1], e, at_y(dy))
+        send(block, block, xe_sem.at[d * 4], e, partner)
+
+    for d in (0,) + NEAR_FIRST:
+        spread(d)
     sq = fsq[...]
     for d in NEAR_FIRST:
         arrived(fsqr.at[d - 1], fs_sem.at[d - 1])
@@ -334,13 +340,37 @@
     row_scale = jnp.sum(jnp.where(own_row, jnp.broadcast_to(inverse, (64, SEQS)), 0.0), axis=1, keepdims=True)
     c_eg.wait()
     c_eu.wait()
-    acc = jnp.zeros((CAP, 256), F32)
+    def product(core, zs):
+        rows = jnp.concatenate([xe[2 * yi + core, zs].astype(F32) for yi in range(4)], axis=0).astype(BF16)
+        both = jnp.concatenate([egb[zs], eub[zs]], axis=1)
+        return jnp.dot(rows, both, preferred_element_type=F32)
+
+    near = jnp.zeros((HALF, 256), F32)
     for d in (0,) + NEAR_FIRST:
         zs = at_z(NZ - d)
-        arrived(xe.at[1 - c, zs], xe_sem.at[d])
-        rows = jnp.concatenate([xe[0, zs], xe[1, zs]], axis=0)
-        both = jnp.concatenate([egb[zs], eub[zs]], axis=1)
-        acc = acc + jnp.dot(rows, both, preferred_element_type=F32)
+        for dy in (1, 3, 2):
+            block = xe.at[at_y(4 - dy), zs]
+            arrived(block, xy_sem.at[d * 3 + dy - 1])
+            send(block, block, xe_sem.at[d * 4 + dy], e, partner)
+        near = near + product(c, zs)
+
+    gu = gub[z].astype(F32)
+    for d in NEAR_FIRST:
+        arrived(gurecv.at[d - 1], gu_sem.at[d - 1])
+        gu = gu + gurecv[d - 1].astype(F32)
+    gu = gu * row_scale
+    gate = gu[:, 0:128]
+    hd[x, z] = (gate / (1.0 + jnp.exp(-gate)) * gu[:, 128:256]).astype(BF16)
+    for d in FAR_FIRST:
+        send(hd.at[x, z], hd.at[x, z], hz_sem.at[d - 1], at_z(d) * NX + x, t)
+
+    across = jnp.zeros((HALF, 256), F32)
+    for d in (0,) + NEAR_FIRST:
+        zs = at_z(NZ - d)
+        for dy in (0, 1, 3, 2):
+            arrived(xe.at[lax.rem(partner + 2 * (4 - dy), NT), zs], xe_sem.at[d * 4 + dy])
+        across = across + product(1 - c, zs)
+    acc = jnp.concatenate([jnp.where(c == 0, near, across), jnp.where(c == 0, across, near)], axis=0)
     acc = acc * slot_scale
     gate = acc[:, 0:128]
     hidden = (gate / (1.0 + jnp.exp(-gate)) * acc[:, 128:256]).astype(BF16)
@@ -356,38 +386,45 @@
             pout[zi, xi] = given[:, xi * 128 : (xi + 1) * 128]
         send(pout.at[zi], precv.at[zi], p_sem.at[k], e, partner)
 
-    gu = gub[z].astype(F32)
-    for d in NEAR_FIRST:
-        arrived(gurecv.at[d - 1], gu_sem.at[d - 1])
-        gu = gu + gurecv[d - 1].astype(F32)
-    gu = gu * row_scale
-    gate = gu[:, 0:128]
-    hd[x, z] = (gate / (1.0 + jnp.exp(-gate)) * gu[:, 128:256]).astype(BF16)
-    for d in FAR_FIRST:
-        send(hd.at[x, z], hd.at[x, z], hz_sem.at[d - 1], at_z(d) * NX + x, t)
-
     for k, d in enumerate(FAR_FIRST + (0,)):
         zi = at_z(d)
         arrived(precv.at[zi], p_sem.at[k])
-        rsum[zi] = (pown[zi].astype(F32) + precv[zi].astype(F32)).astype(BF16)
+        pair = pown[zi].astype(F32) + precv[zi].astype(F32)
+        for yi in range(4):
+            rsum[zi, yi] = jnp.concatenate([pair[xi, yi * 8 : (yi + 1) * 8] for xi in range(NX)], axis=0).astype(BF16)
+        for dy in (2, 1, 3):
+            send(rsum.at[zi, lax.rem(y + dy, 4)], ysum.at[dy - 1, zi], ys_sem.at[k * 3 + dy - 1], e, at_y(dy))
+
+    def onward(d):
+        block = hd.at[x, at_z(NZ - d)]
+        if d:
+            arrived(block, hz_sem.at[d - 1])
+        for dx in (2, 1, 3):
+            send(block, block, hx_sem.at[d * 3 + dx - 1], z * NX + at_x(dx), t)
+
+    for d in (0, 1, 7, 2, 6):
+        onward(d)
+    for k, d in enumerate(FAR_FIRST + (0,)):
+        zi = at_z(d)
+        whole = rsum[zi, y].astype(F32)
+        for dy in (1, 3, 2):
+            arrived(ysum.at[dy - 1, zi], ys_sem.at[k * 3 + dy - 1])
+            whole = whole + ysum[dy - 1, zi].astype(F32)
+        for xi in range(NX):
+            back[zi, xi] = whole[xi * 8 : (xi + 1) * 8].astype(BF16)
         for dx in (2, 1, 3, 0):
             if d or dx:
-                send(rsum.at[zi, at_x(dx)], rt.at[e], rt_sem.at[d * NX + dx], zi * NX + at_x(dx), t)
-    rt[e] = rsum[z, x]
-
-    for dx in (2, 1, 3):
-        send(hd.at[x, z], hd.at[x, z], hx_sem.at[dx - 1], z * NX + at_x(dx), t)
-    for d in NEAR_FIRST:
-        zs = at_z(NZ - d)
-        arrived(hd.at[x, zs], hz_sem.at[d - 1])
-        for dx in (2, 1, 3):
-            send(hd.at[x, zs], hd.at[x, zs], hx_sem.at[d * 3 + dx - 1], z * NX + at_x(dx), t)
+                send(back.at[zi, at_x(dx)], rt.at[e], rt_sem.at[d * NX + dx], zi * NX + at_x(dx), t)
+    rt[e] = back[z, x]
+    for d in (3, 5, 4):
+        onward(d)
 
     for d in range(NZ):
         for dx in range(NX):
             if d or dx:
                 arrived(rt.at[at_z(NZ - d) * NX + at_x(NX - dx)], rt_sem.at[d * NX + dx])
-    moe = lax.dot_general(ctm[...], rt[...].reshape(1024, 128), (((0,), (0,)), ((), ())), preferred_element_type=F32)
+    returned = rt[...].astype(F32).reshape(256, 128).astype(BF16)
+    moe = lax.dot_general(ctm[...], returned, (((0,), (0,)), ((), ())), preferred_element_type=F32)
     for d in (0,) + NEAR_FIRST:
         for dx in (1, 3, 2):
             arrived(hd.at[at_x(NX - dx), at_z(NZ - d)], hx_sem.at[d * 3 + dx - 1])
@@ -448,17 +485,17 @@
         wog=b(NX, 256, 128), hall=b(NZ, ROWS, 256), obuf=b(NZ, ROWS, 512), orecv=b(NT - 1, ROWS, 512),
         sres=b(NX, ROWS, 128), fgb=f(8, 128), fgall=f(NX, 8, 128),
         wgu=b(NX, 128, 256), ddb=b(512, 128), egb=b(NZ, 512, 128), eub=b(NZ, 512, 128), edb=b(NZ, 128, 512),
-        pmat=b(256, SEQS), ctm=b(1024, SEQS), rbuf=b(ROWS, 512), rall=b(NT, NX, ROWS, 512), gbuf=b(SEQS, 512),
+        pmat=b(64, SEQS), ctm=b(256, SEQS), rbuf=b(ROWS, 512), rall=b(NT, NX, ROWS, 512), gbuf=b(SEQS, 512),
         fsq=f(8, 128), fsqr=f(NZ - 1, 8, 128), gub=b(NZ, 64, 256), gurecv=b(NZ - 1, 64, 256),
-        dbuf=b(NZ, HALF, 512), xe=b(2, NZ, HALF, 512), hd=b(NX, NZ, 64, 128),
-        pown=b(NZ, NX, HALF, 128), pout=b(NZ, NX, HALF, 128), precv=b(NZ, NX, HALF, 128), rsum=b(NZ, NX, HALF, 128),
-        rt=b(32, HALF, 128), fbuf=b(2, 256, 128), fpair=b(256, 128), fhalf=b(256, 128), frecv=b(3, 256, 128), mgath=b(2, 256, 128),
-        lsem=dma((32,)), ssem=dma((224,)), ring_sem=pltpu.SemaphoreType.REGULAR((4,)),
+        dbuf=b(NZ, 8, 512), xe=b(NT, NZ, 8, 512), hd=b(NX, NZ, 64, 128),
+        pown=b(NZ, NX, HALF, 128), pout=b(NZ, NX, HALF, 128), precv=b(NZ, NX, HALF, 128), rsum=b(NZ, 4, HALF, 128),
+        ysum=b(3, NZ, HALF, 128), back=b(NZ, NX, 8, 128), rt=b(32, 8, 128), fbuf=b(2, 256, 128), fpair=b(256, 128), fhalf=b(256, 128), frecv=b(3, 256, 128), mgath=b(2, 256, 128),
+        lsem=dma((32,)), ssem=dma((320,)), ring_sem=pltpu.SemaphoreType.REGULAR((4,)),
         yq_sem=dma((24,)), yk_sem=dma((3,)), sx_sem=dma((3,)), wo_sem=dma((3,)), wg_sem=dma((3,)), wu_sem=dma((3,)),
         sr_sem=dma((3,)), fg_sem=dma((3,)), zq_sem=dma((7,)), zk_sem=dma((7,)), sz_sem=dma((7,)), h_sem=dma((7,)), o_sem=dma((7,)),
         r_sem=dma((16,)), rf_sem=dma((16,)),
-        fs_sem=dma((7,)), gu_sem=dma((7,)), d_sem=dma((7,)), xe_sem=dma((8,)), hz_sem=dma((7,)),
-        hx_sem=dma((24,)), p_sem=dma((8,)), rt_sem=dma((32,)), f_sem=dma((4,)), m_sem=dma((1,)),
+        fs_sem=dma((7,)), gu_sem=dma((7,)), d_sem=dma((7,)), xy_sem=dma((24,)), xe_sem=dma((32,)), hz_sem=dma((7,)),
+        hx_sem=dma((24,)), p_sem=dma((8,)), ys_sem=dma((24,)), rt_sem=dma((32,)), f_sem=dma((4,)), m_sem=dma((1,)),
     )
     results = pl.pallas_call(
         step_kernel,

time: 81.4 us -> 77.1 us (0.947)
  Pallas kernels: 80.6 us -> 76.4 us
    pallas_call x1, Pallas kernels: 79 us -> 74.8 us  [per_device(): pl.pallas_call(step_kernel, name='step', out_shape=(jax.ShapeDtypeStruct(...]
where the time goes in v4:
time: 77.1 us; the launch traced here: 77 us
  Pallas kernels  76.4 us (99%)
    pallas_call x1, Pallas kernels, per_device(): pl.pallas_call(step_kernel, name='step', out_shape=(jax.ShapeDtypeStruct(...  74.8 us
    pallas_call x1, Pallas kernels, per_device(): pl.pallas_call(finish_kernel, name='finish', out_shape=tuple((jax.ShapeDt...  1.58 us

profile of v4, /device:TPU:1, one launch (start us, length us, event | category | flops | bytes accessed | tf_op | source)
XLA Modules:
  0.0 77.0 jit_solution(1952254546890625748)
XLA Ops:
  0.6 74.8 %step.1 = (bf16[512,128]{1,0:T(8,128)(2,1)}, bf16[16,128]{1,0:T(8,128)(2,1)}, bf16[16,128]{1,0:T(8,128)(2,1)}) custom-call(bf16[8,4,16,128]{3,2,1,0:T(8,128)(2,1)} %bitcast.17, bf16[128,256]{1,0:T(8,128)(2,1)} %wq.1, bf16[128,128]{1,0:T(8,128)(2,1)} %wk.1, bf16[128,128]{1,0:T(8,128)(2,1)} %wv.1, bf16[16,1024,128]{2,1,0:T(8,128)(2,1)} %bitcast.12, ...), custom_call_target="tpu_custom_call" | custom-call | tf_op jit(solution)/shard_map/step/pallas_call | solution.py:500
  75.5 1.6 %finish.1 = (bf16[512,128]{1,0:T(8,128)(2,1)}, bf16[16,128]{1,0:T(8,128)(2,1)}, bf16[16,128]{1,0:T(8,128)(2,1)}) custom-call(bf16[512,128]{1,0:T(8,128)(2,1)} %get-tuple-element.6.a, bf16[16,128]{1,0:T(8,128)(2,1)} %get-tuple-element.7.b, bf16[16,128]{1,0:T(8,128)(2,1)} %get-tuple-element.8.c), custom_call_target="tpu_custom_call" | custom-call | tf_op jit(solution)/shard_map/finish/pallas_call | solution.py:520

commit v5 on v4

--- a/solution.py
+++ b/solution.py
@@ -28,7 +28,7 @@
     strm, wqkv, kbuf, vbuf, xgain, yq, yqr, yk, ykr, ssq, ssqr, zq, zqr, zk, zkr, zsq, zsqr,
     wog, hall, obuf, orecv, sres, fgb, fgall, wgu, ddb, egb, eub, edb,
     pmat, ctm, rbuf, rall, gbuf, fsq, fsqr, gub, gurecv, dbuf, xe, hd,
-    pown, pout, precv, rsum, ysum, back, rt, fbuf, fpair, fhalf, frecv, mgath,
+    pown, pout, precv, rsum, ysum, back, rt, fbuf, fpair, fhalf, frecv, mgath, kvout,
     lsem, ssem, ring_sem,
     yq_sem, yk_sem, sx_sem, wo_sem, wg_sem, wu_sem, sr_sem, fg_sem, zq_sem, zk_sem, sz_sem, h_sem, o_sem, r_sem, rf_sem,
     fs_sem, gu_sem, d_sem, xy_sem, xe_sem, hz_sem, hx_sem, p_sem, ys_sem, rt_sem, f_sem, m_sem,
@@ -282,8 +282,9 @@
         arrived(zkr.at[d - 1], zk_sem.at[d - 1])
         kv = kv + zkr[d - 1].astype(F32)
     kv = kv * token_scale
-    key_rows[...] = kv[:, 0:128].astype(BF16)
-    value_rows[...] = kv[:, 128:256].astype(BF16)
+    kvout[0] = kv[:, 0:128].astype(BF16)
+    kvout[1] = kv[:, 128:256].astype(BF16)
+    c_out = [load(kvout.at[0], key_rows), load(kvout.at[1], value_rows)]
     for dy in (0, 1, 3, 2):
         for dx in (0, 1, 3, 2):
             if dy or dx:
@@ -295,21 +296,23 @@
         for dx in range(NX):
             arrived(rall.at[lax.rem(other + 2 * (4 - dy), NT), at_x(NX - dx)], rf_sem.at[dy * NX + dx])
     gains = jnp.concatenate([fgall[xi][0:1] for xi in range(NX)], axis=1)
+    for i in range(4):
+        rows = rall[2 * i : 2 * i + 2].reshape(128, 512).astype(F32)
+        gbuf[i * 128 : (i + 1) * 128] = (rows * gains).astype(BF16)
+    dispatched = jnp.dot(pmat[...], gbuf[...], preferred_element_type=F32)
+    dbuf[...] = dispatched.reshape(NZ, 8, 512).astype(BF16)
+    for d in FAR_FIRST:
+        send(dbuf.at[at_z(d)], xe.at[t, z], d_sem.at[d - 1], at_z(d) * NX + x, t)
+    xe[t, z] = dbuf[z]
     square_rows = []
     for i in range(4):
         rows = rall[2 * i : 2 * i + 2].reshape(128, 512).astype(F32)
-        gbuf[i * 128 : (i + 1) * 128] = (rows * gains).astype(BF16)
         squares = rows * rows
         squares = squares[:, 0:128] + squares[:, 128:256] + squares[:, 256:384] + squares[:, 384:512]
         square_rows.append(jnp.sum(squares.T, axis=0, keepdims=True))
     fsq[...] = jnp.concatenate(square_rows + [jnp.zeros((4, 128), F32)], axis=0)
-    dispatched = jnp.dot(pmat[...], gbuf[...], preferred_element_type=F32)
-    dbuf[...] = dispatched.reshape(NZ, 8, 512).astype(BF16)
-    for d in FAR_FIRST:
-        to = at_z(d) * NX + x
-        send(dbuf.at[at_z(d)], xe.at[t, z], d_sem.at[d - 1], to, t)
-        send(fsq, fsqr.at[d - 1], fs_sem.at[d - 1], to, t)
-    xe[t, z] = dbuf[z]
+    for d in FAR_FIRST:
+        send(fsq, fsqr.at[d - 1], fs_sem.at[d - 1], at_z(d) * NX + x, t)
     wide = wgu[...].reshape(512, 256)
     for i in range(4):
         part = jnp.dot(gbuf[i * 128 : (i + 1) * 128], wide, preferred_element_type=F32)
@@ -446,10 +449,12 @@
     for d in (1, 3, 2):
         arrived(frecv.at[d - 1], f_sem.at[d])
         out = out + frecv[d - 1].astype(F32)
-    mgath[c] = out.astype(BF16)
-    send(mgath.at[c], mgath.at[c], m_sem.at[0], e, partner)
-    arrived(mgath.at[1 - c], m_sem.at[0])
-    mixed[...] = mgath[...].reshape(SEQS, 128)
+    mgath[...] = out.astype(BF16)
+    send(mgath, mixed.at[c], m_sem.at[0], e, partner)
+    c_out.append(load(mgath, mixed.at[c]))
+    arrived(mixed.at[1 - c], m_sem.at[0])
+    for copy in c_out:
+        copy.wait()
     for copy in started:
         copy.wait_send()
 
@@ -489,8 +494,8 @@
         fsq=f(8, 128), fsqr=f(NZ - 1, 8, 128), gub=b(NZ, 64, 256), gurecv=b(NZ - 1, 64, 256),
         dbuf=b(NZ, 8, 512), xe=b(NT, NZ, 8, 512), hd=b(NX, NZ, 64, 128),
         pown=b(NZ, NX, HALF, 128), pout=b(NZ, NX, HALF, 128), precv=b(NZ, NX, HALF, 128), rsum=b(NZ, 4, HALF, 128),
-        ysum=b(3, NZ, HALF, 128), back=b(NZ, NX, 8, 128), rt=b(32, 8, 128), fbuf=b(2, 256, 128), fpair=b(256, 128), fhalf=b(256, 128), frecv=b(3, 256, 128), mgath=b(2, 256, 128),
-        lsem=dma((32,)), ssem=dma((320,)), ring_sem=pltpu.SemaphoreType.REGULAR((4,)),
+        ysum=b(3, NZ, HALF, 128), back=b(NZ, NX, 8, 128), rt=b(32, 8, 128), fbuf=b(2, 256, 128), fpair=b(256, 128), fhalf=b(256, 128), frecv=b(3, 256, 128), mgath=b(256, 128), kvout=b(2, ROWS, 128),
+        lsem=dma((40,)), ssem=dma((320,)), ring_sem=pltpu.SemaphoreType.REGULAR((4,)),
         yq_sem=dma((24,)), yk_sem=dma((3,)), sx_sem=dma((3,)), wo_sem=dma((3,)), wg_sem=dma((3,)), wu_sem=dma((3,)),
         sr_sem=dma((3,)), fg_sem=dma((3,)), zq_sem=dma((7,)), zk_sem=dma((7,)), sz_sem=dma((7,)), h_sem=dma((7,)), o_sem=dma((7,)),
         r_sem=dma((16,)), rf_sem=dma((16,)),
@@ -501,12 +506,12 @@
         step_kernel,
         name="step",
         out_shape=(
-            jax.ShapeDtypeStruct((SEQS, 128), BF16),
+            jax.ShapeDtypeStruct((2, 256, 128), BF16),
             jax.ShapeDtypeStruct((ROWS, 128), BF16),
             jax.ShapeDtypeStruct((ROWS, 128), BF16),
         ),
         in_specs=[any_spec] * 21,
-        out_specs=(vm, vm, vm),
+        out_specs=(any_spec,) * 3,
         scratch_shapes=list(scratch.values()),
         compiler_params=pltpu.CompilerParams(collective_id=0, has_side_effects=True, vmem_limit_bytes=60 * 1024 * 1024),
     )(
@@ -517,6 +522,7 @@
         norm_gain.reshape(1, 128), head_gain.reshape(2, 128), ffn_gain.reshape(1, 128), mix_gain.reshape(1, 128),
         route_experts.T, route_weights.T, break_offset, lengths,
     )
+    results = (results[0].reshape(SEQS, 128), results[1], results[2])
     return pl.pallas_call(
         finish_kernel,
         name="finish",

time: 77.1 us -> 76.2 us (0.988)
  Pallas kernels: 76.4 us -> 75.4 us
    pallas_call x1, Pallas kernels: 74.8 us -> 73.8 us  [per_device(): pl.pallas_call(step_kernel, name='step', out_shape=(jax.ShapeDtypeStruct(...]
where the time goes in v5:
time: 76.2 us; the launch traced here: 76.1 us
  Pallas kernels  75.4 us (99%)
    pallas_call x1, Pallas kernels, per_device(): pl.pallas_call(step_kernel, name='step', out_shape=(jax.ShapeDtypeStruct(...  73.8 us
    pallas_call x1, Pallas kernels, per_device(): pl.pallas_call(finish_kernel, name='finish', out_shape=tuple((jax.ShapeDt...  1.58 us

profile of v5, /device:TPU:1, one launch (start us, length us, event | category | flops | bytes accessed | tf_op | source)
XLA Modules:
  0.0 76.1 jit_solution(4542781776224626012)
XLA Ops:
  0.6 73.8 %step.1 = (bf16[2,256,128]{2,1,0:T(8,128)(2,1)}, bf16[16,128]{1,0:T(8,128)(2,1)}, bf16[16,128]{1,0:T(8,128)(2,1)}) custom-call(bf16[8,4,16,128]{3,2,1,0:T(8,128)(2,1)} %bitcast.18, bf16[128,256]{1,0:T(8,128)(2,1)} %wq.1, bf16[128,128]{1,0:T(8,128)(2,1)} %wk.1, bf16[128,128]{1,0:T(8,128)(2,1)} %wv.1, bf16[16,1024,128]{2,1,0:T(8,128)(2,1)} %bitcast.13, ...), custom_call_target="tpu_custom_call" | custom-call | tf_op jit(solution)/shard_map/step/pallas_call | solution.py:505
  74.5 1.6 %finish.1 = (bf16[512,128]{1,0:T(8,128)(2,1)}, bf16[16,128]{1,0:T(8,128)(2,1)}, bf16[16,128]{1,0:T(8,128)(2,1)}) custom-call(bf16[512,128]{1,0:T(8,128)(2,1)} %bitcast.19, bf16[16,128]{1,0:T(8,128)(2,1)} %get-tuple-element.7.b, bf16[16,128]{1,0:T(8,128)(2,1)} %get-tuple-element.8.c), custom_call_target="tpu_custom_call" | custom-call | tf_op jit(solution)/shard_map/finish/pallas_call | solution.py:526
